TPU v7x, 256 devices: a 4x2x16 block of a 4x16x16 slice. The times are simulated.
256 devices in a mesh: grp: 2 (over y), sp: 32 (over z, core), tp: 4 (over x).
Axes of the slice: x: 4, y: 2, z: 16, core: 2. Of those that a mesh axis runs over, the one named last changes fastest.
The devices are a block of a 4x16x16 slice.
Arguments:
- query_rows: bfloat16 [8192, 1024], P(('grp', 'sp'), 'tp'), parts along dimension 0, may hold values from -6 to 6
- key_rows: bfloat16 [8192, 1024], P(('grp', 'sp'), 'tp'), parts along dimension 0, may hold values from -6 to 6
- value_rows: bfloat16 [8192, 1024], P(('grp', 'sp'), 'tp'), parts along dimension 0, may hold values from -6 to 6
- gate_rows: bfloat16 [8192, 1024], P(('grp', 'sp'), 'tp'), parts along dimension 0, may hold values from -6 to 6
- log_decay: float32 [2, 8, 8192], P(None, 'tp', ('grp', 'sp')), parts along dimension 2, may hold values from -2 to 0, as said below
- head_gain: float32 [2, 1024], P(None, 'tp'), may hold values from 0.1 to 1.9
- out_weight: bfloat16 [1024, 2048], P('tp'), may hold values from -0.1875 to 0.1875
- residual: bfloat16 [8192, 2048], P(('grp', 'sp')), parts along dimension 0, may hold values from -6 to 6
- norm_gain: bfloat16 [2048], replicated, may hold values from 0.099609375 to 1.8984375
- gate_weight: bfloat16 [2048, 5632], P('sp', 'tp'), may hold values from -0.125 to 0.125
- up_weight: bfloat16 [2048, 5632], P('sp', 'tp'), may hold values from -0.125 to 0.125
- down_weight: bfloat16 [2048, 5632], P('sp', 'tp'), may hold values from -0.078125 to 0.078125
- gate_taps: bfloat16 [3, 5632], P(None, 'tp'), may hold values from -3.5 to 3.5
- up_taps: bfloat16 [3, 5632], P(None, 'tp'), may hold values from -3.5 to 3.5
Outputs:
- block_out: bfloat16 [8192, 2048], P(('grp', 'sp', 'tp')), parts along dimension 0
There are 2 independent parts, one for each index of `grp`. A program takes and returns all parts, laid end to end along the dimension named above; an argument that names none is the same for every part. Nothing has to cross between parts.
Inputs may be any that keep to these rules, and one draw needn't show every extreme that they name: `log_decay`: every entry is negative.
All inputs are finite; a program needn't handle non-finite values.
Results may differ from a plain program's by a relative error of at most 0.017.
Values may be sent and summed in bfloat16 or wider, within the bound.
A program may use at most 64 MiB of HBM per device.

v0:
```python
import math

import jax
import jax.numpy as jnp
from jax import lax
from jax.sharding import Mesh
from jax.sharding import PartitionSpec as P

HEAD = 128
SP = ("sp_0", "sp_1")
GRP_SP = ("grp", "sp_0", "sp_1")
GRP_SP_TP = ("grp", "sp_0", "sp_1", "tp")


GROUP_EPS = 1e-05
NORM_EPS = 1e-06


def nothing_yet(shard, identity):
    return jax.tree.map(
        lambda a, e: jnp.broadcast_to(jnp.asarray(e, a.dtype), a.shape), shard, identity
    )


def entering_2(shard, axes, combine, identity, reverse):
    before = start = nothing_yet(shard, identity)
    running = shard
    for axis in reversed(axes):
        length, index = (lax.axis_size(axis), lax.axis_index(axis))
        pieces = jax.tree.map(lambda part: lax.all_gather(part, axis), running)
        inside, running = (start, start)
        for k in reversed(range(length)) if reverse else range(length):
            passed = k > index if reverse else k < index
            running = combine(running, jax.tree.map(lambda part: part[k], pieces))
            inside = jax.tree.map(lambda new, old: jnp.where(passed, new, old), running, inside)
        before = combine(inside, before)
    return before


def sent_together(arrays, axis, dim, along):
    ends, at = ([], 0)
    for a in arrays[:-1]:
        at += a.shape[along]
        ends.append(at)
    both = jnp.concatenate(arrays, axis=along)
    return tuple(jnp.split(lax.all_gather(both, axis, axis=dim, tiled=True), ends, axis=along))


def cut_along(shard, dim, length):
    shape = shard.shape
    parts = shard.reshape(*shape[:dim], length, shape[dim] // length, *shape[dim + 1 :])
    return jnp.moveaxis(parts, dim, 0)


def summed_on_arrival(shard, axis, dim):
    parts = cut_along(shard, dim, lax.axis_size(axis))
    arrived = lax.all_to_all(parts, axis, split_axis=0, concat_axis=0, tiled=True)
    return arrived.astype(jnp.float32).sum(axis=0)


def sent_to_all(shard, axis):
    length = lax.axis_size(axis)
    return lax.all_to_all(
        jnp.broadcast_to(shard[None], (length, *shard.shape)), axis, 0, 0, tiled=True
    )


def laid_out(parts, dim):
    parts = jnp.moveaxis(parts, 0, dim)
    shape = parts.shape
    return parts.reshape(*shape[:dim], shape[dim] * shape[dim + 1], *shape[dim + 2 :])


def gathered_copies(shard, axis, dim):
    parts = sent_to_all(shard, axis)
    return laid_out(parts, dim)


def padded_2(shard, sides, width):
    for axis, dim in sides:
        size, length = (lax.axis_size(axis), shard.shape[dim])
        up = [(i, (i + 1) % size) for i in range(size - 1)]
        down = [(j, i) for i, j in up]
        last = lax.slice_in_dim(shard, length - width, length, axis=dim)
        initial = lax.slice_in_dim(shard, 0, width, axis=dim)
        before = lax.ppermute(last, axis, up)
        after = lax.ppermute(initial, axis, down)
        shard = jnp.concatenate([before, shard, after], axis=dim)
    return shard


def state_combine(earlier, later):
    return (earlier[0] * later[0], earlier[1] * later[0][:, None, None] + later[1])


def group_norm(values):
    length, head_count, head_width = values.shape
    centre = values - jnp.mean(values, axis=2, keepdims=True)
    spread = jnp.mean(centre * centre, axis=2, keepdims=True)
    return (centre * lax.rsqrt(spread + GROUP_EPS)).reshape(length, head_count * head_width)


def rms_scale(middle, gain):
    values = middle.astype(jnp.float32)
    multiplier = lax.rsqrt(jnp.mean(values * values, axis=1, keepdims=True) + NORM_EPS)
    return (values * multiplier * gain.astype(jnp.float32)).astype(jnp.bfloat16)


def local_retention(query_all, key_all, value_all, log_rates):
    length, head_count, head_width = query_all.shape
    block_len = math.gcd(length, 512)
    block_count = length // block_len
    cumul = jnp.cumsum(log_rates, axis=1).T
    query_block = query_all.reshape(block_count, block_len, head_count, head_width)
    key_block = key_all.reshape(block_count, block_len, head_count, head_width)
    value_block = value_all.reshape(block_count, block_len, head_count, head_width)
    cumul_block = cumul.reshape(block_count, block_len, head_count)
    before = jnp.concatenate(
        [jnp.zeros((1, head_count), jnp.float32), cumul_block[:-1, -1]], axis=0
    )
    local_cumul = cumul_block - before[:, None, :]
    gap_logs = local_cumul[:, :, None, :] - local_cumul[:, None, :, :]
    lower_mask = (jnp.arange(block_len)[:, None] >= jnp.arange(block_len)[None, :])[
        None, :, :, None
    ]
    decay_mask = jnp.where(lower_mask, jnp.exp(jnp.minimum(gap_logs, 0.0)), 0.0)
    scores = jnp.einsum("bthd,bshd->btsh", query_block, key_block) * decay_mask
    inner_part = jnp.einsum("btsh,bshe->bthe", scores, value_block)
    to_end = jnp.exp(local_cumul[:, -1:, :] - local_cumul)
    block_states = jnp.einsum("bshd,bshe->bhde", key_block * to_end[..., None], value_block)
    block_decay = jnp.exp(local_cumul[:, -1, :])

    def carry_step(carry_state, inputs):
        return (carry_state * inputs[0][:, None, None] + inputs[1], carry_state)

    zero_state = jnp.zeros((head_count, head_width, head_width), jnp.float32)
    end_state, entering = lax.scan(carry_step, zero_state, (block_decay, block_states))
    carried = jnp.einsum("bthd,bhde->bthe", query_block * jnp.exp(local_cumul)[..., None], entering)
    output = (inner_part + carried).reshape(length, head_count, head_width)
    return (output, end_state, cumul, jnp.exp(cumul[-1]))


def with_incoming(output, query_all, cumul, incoming):
    return output + jnp.einsum("thd,hde->the", query_all * jnp.exp(cumul)[:, :, None], incoming)


def shards(
    query_rows,
    key_rows,
    value_rows,
    gate_rows,
    log_decay,
    head_gain,
    out_weight,
    residual,
    norm_gain,
    gate_weight,
    up_weight,
    down_weight,
    gate_taps,
    up_taps,
):
    pair_local = jnp.concatenate([gate_weight, up_weight], axis=1)
    row_count = query_rows.shape[0]
    head_count = query_rows.shape[1] // HEAD
    key_scale = HEAD ** (-0.5)
    query_all = query_rows.astype(jnp.float32).reshape(row_count, head_count, HEAD)
    key_all = key_rows.astype(jnp.float32).reshape(row_count, head_count, HEAD) * key_scale
    value_all = value_rows.astype(jnp.float32).reshape(row_count, head_count, HEAD)
    identity = (
        jnp.ones((head_count,), jnp.float32),
        jnp.zeros((head_count, HEAD, HEAD), jnp.float32),
    )
    ahead_local, ahead_state, ahead_cumul, ahead_decay = local_retention(
        query_all, key_all, value_all, log_decay[0]
    )
    query_back = query_all[::-1]
    behind_local, behind_state, behind_cumul, behind_decay = local_retention(
        query_back, key_all[::-1], value_all[::-1], log_decay[1][:, ::-1]
    )
    ahead_in = entering_2((ahead_decay, ahead_state), SP, state_combine, identity, False)[1]
    behind_in = entering_2((behind_decay, behind_state), SP, state_combine, identity, True)[1]
    ahead_out = with_incoming(ahead_local, query_all, ahead_cumul, ahead_in)
    behind_out = with_incoming(behind_local, query_back, behind_cumul, behind_in)[::-1]
    combined = group_norm(ahead_out) * head_gain[0] + group_norm(behind_out) * head_gain[1]
    mixed_heads = (jax.nn.silu(gate_rows.astype(jnp.float32)) * combined).astype(jnp.bfloat16)
    gathered = sent_together((pair_local, down_weight), SP, 0, 1)
    pair_full, down_full = gathered
    share_rows = row_count // lax.axis_size("tp")
    own_start = lax.axis_index("tp") * share_rows
    picked = mixed_heads
    attended = summed_on_arrival(
        jnp.dot(picked, out_weight, preferred_element_type=jnp.float32).astype(jnp.bfloat16),
        "tp",
        0,
    )
    residual_own = lax.dynamic_slice_in_dim(residual, own_start, share_rows, 0)
    middle_own = lax.optimization_barrier(
        (residual_own.astype(jnp.float32) + attended).astype(jnp.bfloat16)
    )
    normed = rms_scale(middle_own, norm_gain)
    pre_both = jnp.dot(
        gathered_copies(normed, "tp", 0), pair_full, preferred_element_type=jnp.float32
    ).astype(jnp.bfloat16)
    padded = padded_2(pre_both, ((SP, 0),), 1)
    half_width = gate_taps.shape[1]
    tap_table = jnp.concatenate([gate_taps, up_taps], axis=1).astype(jnp.float32)
    conv_out = (
        tap_table[0] * padded[:-2].astype(jnp.float32)
        + tap_table[1] * padded[1:-1].astype(jnp.float32)
        + tap_table[2] * padded[2:].astype(jnp.float32)
    )
    hidden = (jax.nn.silu(conv_out[:, :half_width]) * conv_out[:, half_width:]).astype(jnp.bfloat16)
    picked = hidden
    ff_out = summed_on_arrival(
        lax.dot_general(
            picked, down_full, (((1,), (1,)), ((), ())), preferred_element_type=jnp.float32
        ).astype(jnp.bfloat16),
        "tp",
        0,
    )
    return (middle_own.astype(jnp.float32) + ff_out).astype(jnp.bfloat16)


def solution(mesh):
    split = Mesh(
        mesh.devices.reshape(mesh.shape["grp"], 16, 2, mesh.shape["tp"]),
        ("grp", "sp_0", "sp_1", "tp"),
    )
    placed = (
        P(GRP_SP, "tp"),
        P(GRP_SP, "tp"),
        P(GRP_SP, "tp"),
        P(GRP_SP, "tp"),
        P(None, "tp", GRP_SP),
        P(None, "tp"),
        P("tp", None),
        P(GRP_SP, None),
        P(),
        P(SP, "tp"),
        P(SP, "tp"),
        P(SP, "tp"),
        P(None, "tp"),
        P(None, "tp"),
    )
    return jax.shard_map(
        shards, mesh=split, in_specs=placed, out_specs=P(GRP_SP_TP, None), check_vma=False
    )
```

profile of v0, /device:TPU:33, one launch (start us, length us, event | category | flops | bytes accessed | tf_op | source)
XLA Modules:
  0.0 316.0 jit_solution(3661982202352808028)
XLA Ops:
  6.6 0.8 slice_bitcast_fusion.33
  7.3 0.1 rev.17
  7.4 0.3 reduce_window_sum.18
  7.8 0.2 slice_reduce_fusion
  7.9 0.1 bitcast_exponential_fusion
  8.0 0.2 exponential_reduce_fusion
  8.2 21.9 %all-gather.4 = f32[2,1,2]{2,1,0:T(1,128)S(1)} all-gather(f32[1,1,2]{2,1,0:T(1,128)S(1)} %bitcast.498), channel_id=1, replica_groups=mesh['grp'=2,'sp_0'=16,'sp_1'=2,'tp'=4] {'sp_1'}, dimensions={0}, use_global_device_ids=true | all-gather | bytes 24 | tf_op jit(solution)/shard_map/all_gather | solution.py:30
  30.1 0.9 bitcast_convert_fusion
  31.0 0.1 rev.18
  31.1 0.9 copy.84
  32.1 0.2 reverse.3
  32.3 0.2 convolution_add_fusion.1
  32.4 2.0 all-gather.1
  34.5 0.7 bitcast_add_fusion
  35.2 0.1 all-gather.12.cloned.1.call-update
  35.3 0.1 all-gather.10.cloned.1.call-start
  35.4 0.3 reduce_window_sum.17
  35.7 0.2 exponential_reduce_fusion.1
  35.9 1.9 all-gather.2
  37.7 0.2 slice_reduce_fusion.1
  37.9 0.1 bitcast_exponential_fusion.1
  38.0 0.2 convolution_add_fusion
  38.2 2.0 all-gather
  40.2 0.7 bitcast_add_fusion.2
  41.0 0.1 all-gather.14.cloned.1.call-start
  41.1 0.9 pad_maximum_fusion.2
  42.0 0.1 all-gather.14.cloned.1.call-update
  42.1 0.1 copy.54
  42.3 0.1 rev.16
  42.4 23.7 %all-gather.3 = f32[16,1,2]{2,1,0:T(1,128)S(1)} all-gather(f32[1,1,2]{2,1,0:T(1,128)S(1)} %get-tuple-element.78), channel_id=1, replica_groups=mesh['grp'=2,'sp_0'=16,'sp_1'=2,'tp'=4] {'sp_0'}, dimensions={0}, use_global_device_ids=true | all-gather | bytes 136 | tf_op jit(solution)/shard_map/all_gather | solution.py:30
  66.0 20.6 %all-gather.5 = f32[16,1,2]{2,1,0:T(1,128)S(1)} all-gather(f32[1,1,2]{2,1,0:T(1,128)S(1)} %get-tuple-element.84), channel_id=1, replica_groups=mesh['grp'=2,'sp_0'=16,'sp_1'=2,'tp'=4] {'sp_0'}, dimensions={0}, use_global_device_ids=true | all-gather | bytes 136 | tf_op jit(solution)/shard_map/all_gather | solution.py:30
  86.7 0.2 fusion.197
  87.0 0.2 fusion.194
  87.2 5.4 %all-gather.12.cloned.1.call-done = f32[16,2,128,128]{3,2,1,0:T(8,128)} async-done(((f32[1,2,128,128]{3,2,1,0:T(8,128)}), f32[16,2,128,128]{3,2,1,0:T(8,128)}) %all-gather.12.cloned.1.call-update) | async-done | bytes 2097168 | tf_op jit(solution)/shard_map/all_gather | solution.py:30
  92.6 2.1 convolution_bitcast_fusion
  94.7 0.4 fusion.15
  95.1 0.1 rev.19
  95.2 0.1 reduce_sum.65
  95.3 0.2 multiply_reduce_fusion
  95.5 0.1 subtract_multiply_fusion
  95.7 0.1 copy.73
  95.8 65.3 %all-gather.10.cloned.1.call-done = f32[16,2,128,128]{3,2,1,0:T(8,128)} async-done(((f32[1,2,128,128]{3,2,1,0:T(8,128)}), f32[16,2,128,128]{3,2,1,0:T(8,128)}) %all-gather.10.cloned.1.call-update) | async-done | bytes 2097168 | tf_op jit(solution)/shard_map/all_gather | solution.py:30
  161.0 2.1 convolution_bitcast_fusion.3
  163.2 0.4 fusion.322
  163.7 0.1 fusion.188
  163.8 1.1 convolution_convert_fusion
  165.0 4.0 %all-to-all-start = ((bf16[4,32,2048]{2,1,0:T(8,128)(2,1)}), bf16[4,32,2048]{2,1,0:T(8,128)(2,1)S(1)}, u32[]{:S(2)}, u32[]{:S(2)}) async-start(bf16[4,32,2048]{2,1,0:T(8,128)(2,1)} %bitcast.98), calls=%async_computation | async-start | bytes 1048576 | tf_op jit(solution)/shard_map/all_to_all | solution.py:57
  169.0 6.9 %all-to-all-done = bf16[4,32,2048]{2,1,0:T(8,128)(2,1)S(1)} async-done(((bf16[4,32,2048]{2,1,0:T(8,128)(2,1)}), bf16[4,32,2048]{2,1,0:T(8,128)(2,1)S(1)}, u32[]{:S(2)}, u32[]{:S(2)}) %all-to-all-start) | async-done | bytes 524320 | tf_op jit(solution)/shard_map/all_to_all | solution.py:57
  175.9 0.1 convert_reduce_fusion.1
  176.0 0.9 add_convert_fusion
  176.9 0.1 fusion.23
  177.1 0.1 fusion.25
  177.2 12.1 %all_to_all.15 = bf16[4,32,2048]{2,1,0:T(8,128)(2,1)S(1)} all-to-all(bf16[4,32,2048]{2,1,0:T(8,128)(2,1)S(1)} %broadcast_in_dim.28), channel_id=1, replica_groups=mesh['grp'=2,'sp_0'=16,'sp_1'=2,'tp'=4] {'tp'}, dimensions={0} | all-to-all | bytes 1048576 | tf_op jit(solution)/shard_map/all_to_all | solution.py:63
  189.4 88.3 %all-gather.14.cloned.1.call-done = bf16[2048,4224]{1,0:T(8,128)(2,1)} async-done(((bf16[64,4224]{1,0:T(8,128)(2,1)}), bf16[2048,4224]{1,0:T(8,128)(2,1)}) %all-gather.14.cloned.1.call-update) | async-done | bytes 17301520 | tf_op jit(solution)/shard_map/all_gather | solution.py:46
  277.7 6.0 %fusion.4 = bf16[128,2816]{1,0:T(8,128)(2,1)S(1)} fusion(bf16[128,2048]{1,0:T(8,128)(2,1)S(1)} %bitcast.488, bf16[2048,4224]{1,0:T(8,128)(2,1)} %all-gather.14.cloned.1.call-done), kind=kOutput, calls=%fused_computation.4 | convolution fusion | flops 1476755456 | bytes 12779520 | tf_op jit(solution)/shard_map/dot_general | solution.py:202
  283.8 2.0 collective-permute-start
  285.7 2.4 collective-permute-start.1
  288.2 0.1 convert_reduce_fusion.3
  288.3 2.5 collective-permute-done.1
  290.7 0.5 multiply_add_fusion
  291.2 4.6 %fusion.7 = bf16[128,2048]{1,0:T(8,128)(2,1)S(1)} fusion(bf16[2048,4224]{1,0:T(8,128)(2,1)} %all-gather.14.cloned.1.call-done, f32[128,2816]{1,0:T(8,128)S(1)} %multiply_add_fusion), kind=kOutput, calls=%fused_computation.5 | convolution fusion | flops 739540992 | bytes 7733248 | tf_op jit(solution)/shard_map/dot_general | solution.py:216
  295.9 12.8 %all_to_all.16 = bf16[4,32,2048]{2,1,0:T(8,128)(2,1)S(1)} all-to-all(bf16[4,32,2048]{2,1,0:T(8,128)(2,1)S(1)} %bitcast.489), channel_id=1, replica_groups=mesh['grp'=2,'sp_0'=16,'sp_1'=2,'tp'=4] {'tp'}, dimensions={0} | all-to-all | bytes 1048576 | tf_op jit(solution)/shard_map/all_to_all | solution.py:57
  308.7 0.1 convert_reduce_fusion
  308.8 0.7 fusion.26
  (46 shorter events, 0.3 us)
Async XLA Ops:
  6.5 157.3 %copy-start = (bf16[256,2048]{1,0:T(8,128)(2,1)S(1)}, bf16[256,2048]{1,0:T(8,128)(2,1)}, u32[]{:S(2)}) copy-start(bf16[256,2048]{1,0:T(8,128)(2,1)} %param.20) | copy-start | bytes 3145732
  6.6 31.4 %copy-start.2 = (bf16[128,256]{1,0:T(8,128)(2,1)S(1)}, bf16[128,256]{1,0:T(8,128)(2,1)}, u32[]{:S(2)}) copy-start(bf16[128,256]{1,0:T(8,128)(2,1)} %param.16) | copy-start | bytes 196612
  6.6 86.0 %all-gather.12.cloned.1.call-start = ((), (), s32[]{:S(2)}) async-start(), calls=%async_computation.4 | async-start | bytes 2228224 | tf_op jit(solution)/shard_map/all_gather | solution.py:30
  32.1 9.1 %copy-start.3 = (bf16[64,1408]{1,0:T(8,128)(2,1)S(1)}, bf16[64,1408]{1,0:T(8,128)(2,1)}, u32[]{:S(2)}) copy-start(bf16[64,1408]{1,0:T(8,128)(2,1)} %param.25) | copy-start | bytes 540676
  32.1 9.0 %copy-start.4 = (bf16[64,1408]{1,0:T(8,128)(2,1)S(1)}, bf16[64,1408]{1,0:T(8,128)(2,1)}, u32[]{:S(2)}) copy-start(bf16[64,1408]{1,0:T(8,128)(2,1)} %param.24) | copy-start | bytes 540676
  32.1 9.0 %copy-start.5 = (bf16[64,1408]{1,0:T(8,128)(2,1)S(1)}, bf16[64,1408]{1,0:T(8,128)(2,1)}, u32[]{:S(2)}) copy-start(bf16[64,1408]{1,0:T(8,128)(2,1)} %param.23) | copy-start | bytes 540676
  35.3 125.8 %all-gather.10.cloned.1.call-start = ((), (), s32[]{:S(2)}) async-start(), calls=%async_computation.3 | async-start | bytes 2228224 | tf_op jit(solution)/shard_map/all_gather | solution.py:30
  38.0 4.1 %copy-start.6 = (bf16[128,256]{1,0:T(8,128)(2,1)S(1)}, bf16[128,256]{1,0:T(8,128)(2,1)}, u32[]{:S(2)}) copy-start(bf16[128,256]{1,0:T(8,128)(2,1)} %param.17) | copy-start | bytes 196612
  38.2 4.1 %copy-start.1 = (bf16[128,256]{1,0:T(8,128)(2,1)S(1)}, bf16[128,256]{1,0:T(8,128)(2,1)}, u32[]{:S(2)}) copy-start(bf16[128,256]{1,0:T(8,128)(2,1)} %param.14) | copy-start | bytes 196612
  40.2 46.5 %copy-start.10 = (f32[2,256]{1,0:T(2,128)S(1)}, f32[2,256]{1,0:T(2,128)}, u32[]{:S(2)}) copy-start(f32[2,256]{1,0:T(2,128)} %param.19) | copy-start | bytes 6148
  41.0 236.7 %all-gather.14.cloned.1.call-start = ((), (), s32[]{:S(2)}) async-start(), calls=%async_computation.5 | async-start | bytes 17842176 | tf_op jit(solution)/shard_map/all_gather | solution.py:46
  163.8 5.1 %copy-start.9 = (bf16[2048]{0:T(1024)(128)(2,1)S(1)}, bf16[2048]{0:T(1024)(128)(2,1)}, u32[]{:S(2)}) copy-start(bf16[2048]{0:T(1024)(128)(2,1)} %param.22) | copy-start | bytes 12292
  165.0 10.9 %all-to-all-start = ((bf16[4,32,2048]{2,1,0:T(8,128)(2,1)}), bf16[4,32,2048]{2,1,0:T(8,128)(2,1)S(1)}, u32[]{:S(2)}, u32[]{:S(2)}) async-start(bf16[4,32,2048]{2,1,0:T(8,128)(2,1)} %bitcast.98), calls=%async_computation | async-start | bytes 1048576 | tf_op jit(solution)/shard_map/all_to_all | solution.py:57
  277.7 10.4 %copy-start.7 = (bf16[3,1408]{1,0:T(4,128)(2,1)S(1)}, bf16[3,1408]{1,0:T(4,128)(2,1)}, u32[]{:S(2)}) copy-start(bf16[3,1408]{1,0:T(4,128)(2,1)} %param.27) | copy-start | bytes 25348
  277.7 10.4 %copy-start.8 = (bf16[3,1408]{1,0:T(4,128)(2,1)S(1)}, bf16[3,1408]{1,0:T(4,128)(2,1)}, u32[]{:S(2)}) copy-start(bf16[3,1408]{1,0:T(4,128)(2,1)} %param.26) | copy-start | bytes 25348
  283.8 4.5 %collective-permute-start = (bf16[1,2816]{1,0:T(2,128)(2,1)S(1)}, bf16[1,2816]{1,0:T(2,128)(2,1)S(1)}, u32[]{:S(2)}, u32[]{:S(2)}) collective-permute-start(bf16[1,2816]{1,0:T(2,128)(2,1)S(1)} %get-tuple-element.31), channel_id=1, source_target_pairs={{0,4},{4,8},{8,12},{12,16},{16,20},{20,24},{24,28},{28,32},{32,36}... | collective-permute-start | bytes 16904 | tf_op jit(solution)/shard_map/ppermute | solution.py:86
  285.7 5.0 %collective-permute-start.1 = (bf16[1,2816]{1,0:T(2,128)(2,1)S(1)}, bf16[1,2816]{1,0:T(2,128)(2,1)S(1)}, u32[]{:S(2)}, u32[]{:S(2)}) collective-permute-start(bf16[1,2816]{1,0:T(2,128)(2,1)S(1)} %get-tuple-element.32), channel_id=1, source_target_pairs={{4,0},{8,4},{12,8},{16,12},{20,16},{24,20},{28,24},{32,28},{36,32}... | collective-permute-start | bytes 16904 | tf_op jit(solution)/shard_map/ppermute | solution.py:87
Sparse Core Ops, SparseCore 0:
  35.4 57.1 all-gather.11
  94.4 66.6 all-gather.9
  162.9 114.7 all-gather.13
where the time goes:
time: 317 us; the launch traced here: 316 us
  waiting for transfers between devices  169 us (53%)
  blocking collectives  97.2 us (31%)
  matrix products  17.6 us (6%)
  between operations  13.6 us (4%)
  starting transfers between devices  8.5 us (3%)
  other arithmetic  6.44 us (2%)
  local copies, waits for them, and re-layouts  4.2 us (1%)
    all_gather x1, waiting for transfers between devices, sent_together(): lax.all_gather(both, axis, axis=dim, tiled=True)  88.3 us
    all_gather x6, blocking collectives, entering_2(): pieces = jax.tree.map(lambda part: lax.all_gather(part, axis), running)  72.2 us
    all_gather x2, waiting for transfers between devices, entering_2(): pieces = jax.tree.map(lambda part: lax.all_gather(part, axis), running)  70.7 us
    all_to_all x1, blocking collectives, summed_on_arrival(): lax.all_to_all(parts, axis, split_axis=0, concat_axis=0, tiled=True)  12.8 us
    all_to_all x1, blocking collectives, sent_to_all(): lax.all_to_all(jnp.broadcast_to(shard[None], (length, *shard.shape)), axi...  12.1 us
    all_to_all x1, waiting for transfers between devices, summed_on_arrival(): lax.all_to_all(parts, axis, split_axis=0, concat_axis=0, tiled=True)  6.93 us
  transfers between devices with their start and end apart: 6, of which 5 were waited for; matrix products, arithmetic and copies ran while one was open for 4% of the time, Pallas kernels for 0%

commit v1 on v0

v1 whole, which is shorter than its diff:
```python
import functools

import jax
import jax.numpy as jnp
from jax import lax
from jax.experimental import pallas as pl
from jax.experimental.pallas import tpu as pltpu
from jax.sharding import PartitionSpec as P

HEAD = 128
LANE = 128
GROUP_EPS = 1e-05
NORM_EPS = 1e-06
MESH = pl.DeviceIdType.MESH
F32 = jnp.float32
BF16 = jnp.bfloat16


def nt(a, b):
    return lax.dot_general(a, b, (((1,), (1,)), ((), ())), preferred_element_type=F32)


def tn(a, b):
    return lax.dot_general(a, b, (((0,), (0,)), ((), ())), preferred_element_type=F32)


def nn(a, b):
    return jnp.dot(a, b, preferred_element_type=F32)


class Place:
    def __init__(self, groups, spans, peers):
        self.spans, self.peers, self.chips = spans, peers, spans // 2
        self.sp = lax.axis_index("sp")
        self.tp = lax.axis_index("tp")
        self.core = lax.rem(self.sp, 2)
        self.z = lax.div(self.sp, 2)
        self.paired = groups % 2 == 0
        grp = lax.axis_index("grp")
        self.side = lax.rem(grp, 2)
        self.pair = {"grp": grp + 1 - 2 * self.side}
        self.twin = {"sp": self.sp + 1 - 2 * self.core}

    def chip(self, step):
        return lax.rem(self.z + step + self.chips, self.chips)

    def along(self, step):
        return {"sp": 2 * self.chip(step) + self.core}

    def span(self, step):
        return lax.rem(self.sp + step + self.spans, self.spans)

    def peer(self, step):
        return lax.rem(self.tp + step, self.peers)

    def slot_chip(self, slot):
        step = (slot + 1) // 2
        return self.chip(-step if slot % 2 else step)


def remote(src, dst, send_sem, recv_sem, device):
    return pltpu.make_async_remote_copy(
        src_ref=src, dst_ref=dst, send_sem=send_sem, recv_sem=recv_sem, device_id=device, device_id_type=MESH
    )


class Stream:
    def __init__(self, place, buf, halves, sems):
        self.p, self.buf, self.halves = place, buf, halves
        self.ring_s, self.ring_r, self.pair_s, self.pair_r, self.twin_s, self.twin_r, self.twin2_s, self.twin2_r = sems
        width = buf.shape[1]
        tiles = width // LANE
        ring = round(2 * tiles / 3) if place.paired else tiles
        self.width = width
        self.ring_w = ring * LANE
        self.pair_w = width - self.ring_w
        self.ring_o = pl.multiple_of(place.side * self.pair_w, LANE) if place.paired else 0
        self.pair_o = pl.multiple_of((1 - place.side) * self.ring_w, LANE)
        self.give_o = pl.multiple_of(place.side * self.ring_w, LANE)
        self.block = buf.shape[0] // place.spans
        self.rows = self.block // halves
        self.last = place.chips // 2
        self.opposite = place.chips - 1
        self.started = []
        self.handed = {0}

    def view(self, slot, half, cols, core=None):
        core = self.p.core if core is None else core
        start = pl.multiple_of(slot * 2 * self.block + core * self.block + half * self.rows, self.rows)
        return self.buf.at[pl.ds(start, self.rows), cols]

    def ring_cols(self):
        return pl.ds(self.ring_o, self.ring_w)

    def send(self, src, dst, s, r, device):
        copy = remote(src, dst, s, r, device)
        copy.start()
        self.started.append(copy)

    def to_twin(self, slot, half, cols, s, r):
        view = self.view(slot, half, cols)
        self.send(view, view, s.at[slot, half], r.at[slot, half], self.p.twin)

    def to_pair(self, slot, half):
        if self.p.paired:
            view = self.view(slot, half, pl.ds(self.give_o, self.pair_w))
            self.send(view, view, self.pair_s.at[slot, half], self.pair_r.at[slot, half], self.p.pair)

    def own(self, half):
        cols = self.ring_cols()
        src = self.view(0, half, cols)
        self.send(src, self.view(1, half, cols), self.ring_s.at[0, half], self.ring_r.at[1, half], self.p.along(1))
        self.send(
            src, self.view(2, half, cols), self.ring_s.at[self.opposite, half], self.ring_r.at[2, half], self.p.along(-1)
        )
        self.to_twin(0, half, pl.ds(0, self.width), self.twin_s, self.twin_r)

    def got(self, slot, half):
        view = self.view(slot, half, self.ring_cols())
        remote(view, view, self.ring_s.at[slot, half], self.ring_r.at[slot, half], self.p.along(1)).wait_recv()

    def tick(self, step, half):
        cols = self.ring_cols()
        if step == self.last:
            slots = (self.opposite,)
            self.got(self.opposite, half)
        else:
            behind, ahead = slots = (2 * step - 1, 2 * step)
            if step + 1 < self.last:
                for slot, way in ((behind, 1), (ahead, -1)):
                    self.got(slot, half)
                    self.send(
                        self.view(slot, half, cols),
                        self.view(slot + 2, half, cols),
                        self.ring_s.at[slot, half],
                        self.ring_r.at[slot + 2, half],
                        self.p.along(way),
                    )
            else:
                self.got(behind, half)
                self.got(ahead, half)
                slot = behind + self.p.core
                self.send(
                    self.view(slot, half, cols),
                    self.view(self.opposite, half, cols),
                    self.ring_s.at[slot, half],
                    self.ring_r.at[self.opposite, half],
                    self.p.along(1 - 2 * self.p.core),
                )
        for slot in slots:
            self.to_pair(slot, half)
            self.to_twin(slot, half, cols, self.twin_s, self.twin_r)

    def pair_tick(self, step, half):
        slots = (self.opposite,) if step == self.last else (2 * step - 1, 2 * step)
        if half == self.halves - 1:
            self.handed.update(slots)
        if not self.p.paired:
            return
        cols = pl.ds(self.pair_o, self.pair_w)
        for slot in slots:
            view = self.view(slot, half, cols)
            remote(view, view, self.pair_s.at[slot, half], self.pair_r.at[slot, half], self.p.pair).wait_recv()
            self.to_twin(slot, half, cols, self.twin2_s, self.twin2_r)

    def ready(self, slot):
        for half in range(self.halves):
            cols = pl.ds(0, self.width) if slot == 0 else self.ring_cols()
            view = self.view(slot, half, cols, 1 - self.p.core)
            remote(view, view, self.twin_s.at[slot, half], self.twin_r.at[slot, half], self.p.twin).wait_recv()
            if self.p.paired and slot > 0:
                view = self.view(slot, half, pl.ds(self.pair_o, self.pair_w), 1 - self.p.core)
                remote(view, view, self.twin2_s.at[slot, half], self.twin2_r.at[slot, half], self.p.twin).wait_recv()

    def drain(self):
        for copy in self.started:
            copy.wait_send()


def order(gate_up, down, last, lag):
    late = []

    def one(stream, step, half):
        stream.tick(step, half)
        late.append((stream, step, half))

    for step in range(1, last + lag + 1):
        for half in range(gate_up.halves):
            if step <= last:
                while len(late) > 1:
                    a, b, c = late.pop(0)
                    a.pair_tick(b, c)
                one(gate_up, step, half)
                yield
        for half in range(down.halves):
            if step == lag:
                down.own(half)
            elif step > lag:
                while len(late) > 1:
                    a, b, c = late.pop(0)
                    a.pair_tick(b, c)
                one(down, step - lag, half)
                yield
    for a, b, c in late:
        a.pair_tick(b, c)


def all_to_all(place, src, dst, send_sem, recv_sem):
    spans = place.spans

    def body(t, _):
        step = spans // 2 + (1 - 2 * lax.rem(t, 2)) * lax.div(t + 1, 2)
        to = lax.rem(place.sp + step, spans)
        for s, d, ss, rs in zip(src(to), dst(place.sp), send_sem, recv_sem):
            remote(s, d, ss, rs, {"sp": to}).start()
        return 0

    lax.fori_loop(0, spans - 1, body, 0)


def wait_bytes(view, sem):
    pltpu.make_async_copy(view, view, sem).wait()


def layer(
    groups, spans, peers,
    q_ref, k_ref, v_ref, g_ref, ld_ref, hg_ref, wo_hbm, res_hbm, ng_ref, gw_hbm, uw_hbm, dw_hbm, gt_ref, ut_ref,
    out_ref,
    gu, dn, wo, res, st_send, st_recv, dec_send, dec_recv, in_send, in_recv, inner, grow, mix, att, att_r,
    mid, nsend, nall, nperm, pre, halo_s, halo_r, hid, ff, ff_r,
    load_sem, a2a_s, a2a_r, rs1_s, rs1_r, ag_s, ag_r, halo_ss, halo_rs, rs2_s, rs2_r,
    g0, g1, g2, g3, g4, g5, g6, g7, d0, d1, d2, d3, d4, d5, d6, d7,
):
    place = Place(groups, spans, peers)
    sp, tp, core = place.sp, place.tp, place.core
    length = q_ref.shape[0]
    heads = q_ref.shape[1] // HEAD
    combos = 2 * heads
    share = length // peers
    half_w = gw_hbm.shape[1]
    block = gw_hbm.shape[0]
    slots = place.chips
    scale = HEAD ** (-0.5)

    barrier = pltpu.get_barrier_semaphore()

    def greet(step, _):
        pl.semaphore_signal(barrier, inc=1, device_id={"sp": place.span(step)}, device_id_type=MESH)
        return 0

    pl.semaphore_signal(barrier, inc=1, device_id=place.along(1), device_id_type=MESH)
    pl.semaphore_signal(barrier, inc=1, device_id=place.along(-1), device_id_type=MESH)
    lax.fori_loop(3, spans - 2, greet, 0)
    for step in (1, 2 * 0 + spans - 1):
        pl.semaphore_signal(barrier, inc=1, device_id={"sp": place.span(step)}, device_id_type=MESH)
    greeted = spans - 1
    for step in range(1, peers):
        pl.semaphore_signal(barrier, inc=1, device_id={"tp": place.peer(step)}, device_id_type=MESH)
    greeted += peers - 1
    if place.paired:
        pl.semaphore_signal(barrier, inc=1, device_id=place.pair, device_id_type=MESH)
        greeted += 1

    own_rows = pl.ds(pl.multiple_of(core * block, block), block)
    loads = [
        pltpu.make_async_copy(gw_hbm, gu.at[own_rows, pl.ds(0, half_w)], load_sem.at[0]),
        pltpu.make_async_copy(uw_hbm, gu.at[own_rows, pl.ds(half_w, half_w)], load_sem.at[1]),
        pltpu.make_async_copy(dw_hbm, dn.at[own_rows, :], load_sem.at[2]),
        pltpu.make_async_copy(wo_hbm, wo, load_sem.at[3]),
        pltpu.make_async_copy(res_hbm.at[pl.ds(pl.multiple_of(tp * share, share), share), :], res, load_sem.at[4]),
    ]
    for copy in loads:
        copy.start()

    row = lax.broadcasted_iota(jnp.int32, (HEAD, LANE), 0)
    lane = lax.broadcasted_iota(jnp.int32, (HEAD, LANE), 1)
    rates = [ld_ref[d, pl.ds(h, 1), :] for h in range(heads) for d in range(2)]
    sums = jnp.concatenate(rates + rates[: (-combos) % 8], axis=0) if combos % 8 else jnp.concatenate(rates, axis=0)
    s_lane = lax.broadcasted_iota(jnp.int32, sums.shape, 1)
    s_row = lax.broadcasted_iota(jnp.int32, sums.shape, 0)
    back = (s_row & 1) == 1
    shift = 1
    while shift < length:
        fwd = jnp.where(s_lane >= shift, pltpu.roll(sums, shift, 1), 0.0)
        bwd = jnp.where(s_lane < length - shift, pltpu.roll(sums, length - shift, 1), 0.0)
        sums = sums + jnp.where(back, bwd, fwd)
        shift *= 2
    part = spans // combos
    rows = HEAD // part
    for h in range(heads):
        cols = pl.ds(h * HEAD, HEAD)
        q, k, v = q_ref[:, cols], k_ref[:, cols], v_ref[:, cols]
        v32 = v.astype(F32)
        scores = nt(q, k) * scale
        for d in range(2):
            m = 2 * h + d
            along_s = jnp.broadcast_to(sums[m : m + 1, :], (length, LANE))
            along_t = along_s.T
            seen = (row >= lane) if d == 0 else (row <= lane)
            decay = jnp.where(seen, jnp.exp(jnp.minimum(along_t - along_s, 0.0)), 0.0)
            inner[m] = nn((scores * decay).astype(BF16), v)
            grow[m] = jnp.exp(along_t) * scale
            total = along_t[length - 1 : length, :] if d == 0 else along_t[0:1, :]
            dec_send[m] = jnp.exp(total)
            faded = (v32 * jnp.exp(jnp.minimum(total - along_t, 0.0))).astype(BF16)
            st_send[pl.ds(m * part, part)] = tn(k, faded).astype(BF16).reshape(part, rows, HEAD)

    gate_up = Stream(place, gu, 2, (g0, g1, g2, g3, g4, g5, g6, g7))
    down = Stream(place, dn, 2, (d0, d1, d2, d3, d4, d5, d6, d7))
    ring = order(gate_up, down, place.chips // 2, 2)

    def advance(n):
        for _ in range(n):
            next(ring, None)

    def ready(stream, first, end):
        for slot in range(first, end):
            while slot not in stream.handed:
                next(ring, None)
            stream.ready(slot)

    for copy in loads[:3]:
        copy.wait()
    pl.semaphore_wait(barrier, greeted)

    all_to_all(
        place,
        lambda to: (st_send.at[to], dec_send.at[lax.div(to, part)]),
        lambda me: (st_recv.at[me], dec_recv.at[me]),
        (a2a_s.at[0], a2a_s.at[1]),
        (a2a_r.at[0], a2a_r.at[1]),
    )
    gate_up.own(0)
    gate_up.own(1)
    my_combo = lax.div(sp, part)
    st_recv[pl.ds(sp, 1)] = st_send[pl.ds(sp, 1)]
    dec_recv[pl.ds(sp, 1)] = dec_send[pl.ds(my_combo, 1)]
    advance(ADVANCE[0])
    others = pl.ds(0, spans - 1)
    wait_bytes(st_recv.at[others], a2a_r.at[0])
    wait_bytes(dec_recv.at[others], a2a_r.at[1])

    reverse = lax.rem(my_combo, 2)

    def scan(j, carry):
        at = j + reverse * (spans - 1 - 2 * j)
        in_send[at] = carry.astype(BF16)
        return carry * dec_recv[at] + st_recv[at].astype(F32)

    lax.fori_loop(0, spans, scan, jnp.zeros((rows, HEAD), F32))
    all_to_all(
        place, lambda to: (in_send.at[to],), lambda me: (in_recv.at[me],), (a2a_s.at[2],), (a2a_r.at[2],)
    )
    in_recv[pl.ds(sp, 1)] = in_send[pl.ds(sp, 1)]
    advance(ADVANCE[1])
    for copy in loads[3:]:
        copy.wait()
    wait_bytes(in_recv.at[others], a2a_r.at[2])

    def normed_head(x):
        centre = x - jnp.mean(x, axis=1, keepdims=True)
        spread = jnp.mean(centre * centre, axis=1, keepdims=True)
        return centre * lax.rsqrt(spread + GROUP_EPS)

    for h in range(heads):
        cols = pl.ds(h * HEAD, HEAD)
        q = q_ref[:, cols]
        combined = None
        for d in range(2):
            m = 2 * h + d
            state = in_recv[pl.ds(m * part, part)].reshape(HEAD, HEAD)
            term = normed_head(inner[m] + grow[m] * nn(q, state)) * hg_ref[pl.ds(d, 1), cols]
            combined = term if combined is None else combined + term
        gate = g_ref[:, cols].astype(F32)
        mix[:, cols] = (gate / (1.0 + jnp.exp(-gate)) * combined).astype(BF16)

    width = wo.shape[1]
    tile = min(512, width)
    for n in range(width // tile):
        cols = pl.ds(n * tile, tile)
        att[:, cols] = nn(mix[...], wo[:, cols]).astype(BF16)

    def peer_rows(j):
        return pl.ds(pl.multiple_of(j * share, share), share)

    started = []

    def to_peers(src, dst, s, r):
        for step in range(1, peers):
            copy = remote(src(place.peer(step)), dst(step), s.at[step - 1], r.at[step - 1], {"tp": place.peer(step)})
            copy.start()
            started.append(copy)

    to_peers(lambda j: att.at[peer_rows(j), :], lambda step: att_r.at[step - 1], rs1_s, rs1_r)
    advance(ADVANCE[2])
    for step in range(1, peers):
        remote(att_r.at[step - 1], att_r.at[step - 1], rs1_s.at[step - 1], rs1_r.at[step - 1], {"tp": tp}).wait_recv()
    total = att[peer_rows(tp), :].astype(F32)
    for step in range(1, peers):
        total = total + att_r[step - 1].astype(F32)
    middle = (res[...].astype(F32) + total).astype(BF16)
    mid[...] = middle
    values = middle.astype(F32)
    multiplier = lax.rsqrt(jnp.mean(values * values, axis=1, keepdims=True) + NORM_EPS)
    normed = (values * multiplier * ng_ref[...].astype(F32)).astype(BF16)
    nsend[...] = normed
    nall[peer_rows(tp), :] = normed
    to_peers(lambda j: nsend, lambda step: nall.at[peer_rows(tp), :], ag_s, ag_r)
    advance(ADVANCE[3])
    for step in range(1, peers):
        view = nall.at[peer_rows(place.peer(peers - step)), :]
        remote(view, view, ag_s.at[step - 1], ag_r.at[step - 1], {"tp": tp}).wait_recv()
    for slot in range(slots):
        start = pl.multiple_of(place.slot_chip(slot) * LANE, LANE)
        nperm[:, pl.ds(slot * LANE, LANE)] = nall[:, pl.ds(start, LANE)]

    advance(ADVANCE[4])
    ready(gate_up, 0, slots)

    n_tile = 256 if (2 * half_w) % 256 == 0 else 128

    def project(n, _):
        cols = pl.ds(pl.multiple_of(n * n_tile, n_tile), n_tile)
        pre[:, cols] = nn(nperm[...], gu[:, cols]).astype(BF16).astype(F32)
        return 0

    lax.fori_loop(0, 2 * half_w // n_tile, project, 0)
    halo_s[0] = pre[0:1, :]
    halo_s[1] = pre[length - 1 : length, :]
    before, after = {"sp": place.span(-1)}, {"sp": place.span(1)}
    halos = [
        remote(halo_s.at[0], halo_r.at[1], halo_ss.at[0], halo_rs.at[1], before),
        remote(halo_s.at[1], halo_r.at[0], halo_ss.at[1], halo_rs.at[0], after),
    ]
    for copy in halos:
        copy.start()
    advance(ADVANCE[5])
    for copy in halos:
        copy.wait_recv()
    not_first = (sp > 0).astype(F32)
    not_last = (sp < spans - 1).astype(F32)

    def conv(n, _):
        results = []
        for base, taps in ((0, gt_ref), (half_w, ut_ref)):
            cols = pl.ds(pl.multiple_of(base + n * LANE, LANE), LANE)
            x = pre[:, cols]
            above = jnp.where(row == 0, halo_r[0, :, cols] * not_first, pltpu.roll(x, 1, 0))
            below = jnp.where(row == length - 1, halo_r[1, :, cols] * not_last, pltpu.roll(x, length - 1, 0))
            t = taps[:, pl.ds(pl.multiple_of(n * LANE, LANE), LANE)].astype(F32)
            results.append(t[0:1] * above + t[1:2] * x + t[2:3] * below)
        gate, up = results
        hid[:, pl.ds(pl.multiple_of(n * LANE, LANE), LANE)] = (gate / (1.0 + jnp.exp(-gate)) * up).astype(BF16)
        return 0

    lax.fori_loop(0, half_w // LANE, conv, 0)

    cut = slots // 2
    for part_no, (lo, hi) in enumerate(((0, cut), (cut, slots))):
        ready(down, lo, hi)

        def project_down(n, _):
            rows_ = pl.ds(pl.multiple_of(n * 2 * LANE, 2 * LANE), 2 * LANE)
            ff[:, rows_] = nt(hid[...], dn[rows_, :]).astype(BF16)
            return 0

        lax.fori_loop(lo // 2, hi // 2, project_down, 0)
        cols = pl.ds(lo * LANE, (hi - lo) * LANE)
        to_peers(
            lambda j: ff.at[peer_rows(j), cols],
            lambda step: ff_r.at[step - 1, :, cols],
            rs2_s.at[part_no],
            rs2_r.at[part_no],
        )
    for part_no, (lo, hi) in enumerate(((0, cut), (cut, slots))):
        cols = pl.ds(lo * LANE, (hi - lo) * LANE)
        for step in range(1, peers):
            view = ff_r.at[step - 1, :, cols]
            remote(view, view, rs2_s.at[part_no, step - 1], rs2_r.at[part_no, step - 1], {"tp": tp}).wait_recv()
        for slot in range(lo, hi):
            held = pl.ds(slot * LANE, LANE)
            home = pl.ds(pl.multiple_of(place.slot_chip(slot) * LANE, LANE), LANE)
            total = ff[peer_rows(tp), held].astype(F32)
            for step in range(1, peers):
                total = total + ff_r[step - 1, :, held].astype(F32)
            out_ref[:, home] = (mid[:, home].astype(F32) + total).astype(BF16)

    advance(10_000)
    for copy in started + halos:
        copy.wait_send()
    wait_bytes(st_send.at[others], a2a_s.at[0])
    wait_bytes(dec_recv.at[others], a2a_s.at[1])
    wait_bytes(in_send.at[others], a2a_s.at[2])
    gate_up.drain()
    down.drain()


ADVANCE = (3, 3, 4, 5, 10, 3)


def solution(mesh):
    groups, spans, peers = mesh.shape["grp"], mesh.shape["sp"], mesh.shape["tp"]
    rows_, cols_ = ("grp", "sp"), "tp"
    placed = (
        P(rows_, cols_), P(rows_, cols_), P(rows_, cols_), P(rows_, cols_), P(None, cols_, rows_), P(None, cols_),
        P(cols_, None), P(rows_, None), P(), P("sp", cols_), P("sp", cols_), P("sp", cols_), P(None, cols_),
        P(None, cols_),
    )

    def shards(q, k, v, g, ld, hg, wo, res, ng, gw, uw, dw, gt, ut):
        length = q.shape[0]
        heads = q.shape[1] // HEAD
        combos = 2 * heads
        share = length // peers
        block, half_w = gw.shape
        width = wo.shape[1]
        chips = spans // 2
        packet = HEAD * combos // spans
        dma = pltpu.SemaphoreType.DMA
        vmem = pl.BlockSpec(memory_space=pltpu.VMEM)
        any_ = pl.BlockSpec(memory_space=pl.ANY)
        scratch = [
            pltpu.VMEM((spans * block, 2 * half_w), BF16),
            pltpu.VMEM((spans * block, half_w), BF16),
            pltpu.VMEM(wo.shape, BF16),
            pltpu.VMEM((share, width), BF16),
            pltpu.VMEM((spans, packet, HEAD), BF16),
            pltpu.VMEM((spans, packet, HEAD), BF16),
            pltpu.VMEM((combos, 1, LANE), F32),
            pltpu.VMEM((spans, 1, LANE), F32),
            pltpu.VMEM((spans, packet, HEAD), BF16),
            pltpu.VMEM((spans, packet, HEAD), BF16),
            pltpu.VMEM((combos, length, HEAD), F32),
            pltpu.VMEM((combos, length, HEAD), F32),
            pltpu.VMEM((length, heads * HEAD), BF16),
            pltpu.VMEM((length, width), BF16),
            pltpu.VMEM((peers - 1, share, width), BF16),
            pltpu.VMEM((share, width), BF16),
            pltpu.VMEM((share, width), BF16),
            pltpu.VMEM((length, width), BF16),
            pltpu.VMEM((length, width), BF16),
            pltpu.VMEM((length, 2 * half_w), F32),
            pltpu.VMEM((2, 1, 2 * half_w), F32),
            pltpu.VMEM((2, 1, 2 * half_w), F32),
            pltpu.VMEM((length, half_w), BF16),
            pltpu.VMEM((length, width), BF16),
            pltpu.VMEM((peers - 1, share, width), BF16),
            dma((5,)), dma((3,)), dma((3,)), dma((peers - 1,)), dma((peers - 1,)), dma((peers - 1,)), dma((peers - 1,)),
            dma((2,)), dma((2,)), dma((2, peers - 1)), dma((2, peers - 1)),
        ] + [dma((chips, 2)) for _ in range(16)]
        return pl.pallas_call(
            functools.partial(layer, groups, spans, peers),
            name="layer",
            out_shape=jax.ShapeDtypeStruct((share, width), BF16),
            in_specs=[vmem] * 6 + [any_, any_, vmem, any_, any_, any_, vmem, vmem],
            out_specs=vmem,
            scratch_shapes=scratch,
            compiler_params=pltpu.CompilerParams(
                collective_id=0, has_side_effects=True, vmem_limit_bytes=50 * 1024 * 1024
            ),
        )(q, k, v, g, ld, hg, wo, res, ng.reshape(1, -1), gw, uw, dw, gt, ut)

    return jax.shard_map(shards, mesh=mesh, in_specs=placed, out_specs=P(("grp", "sp", "tp"), None), check_vma=False)
```

time: 317 us -> 142 us (0.45)
  waiting for transfers between devices: 169 us -> 0 us
  Pallas kernels: 0 us -> 129 us
  blocking collectives: 97.2 us -> 0 us
  matrix products: 17.6 us -> 0 us
  between operations: 13.6 us -> 0.03 us
  starting transfers between devices: 8.5 us -> 0 us
  local copies, waits for them, and re-layouts: 4.2 us -> 11.8 us
  other arithmetic: 6.44 us -> 0 us
    all_gather x3 -> x0, waiting for transfers between devices: 159 us -> none  [the longest x1 88.3 us: sent_together(): lax.all_gather(both, axis, axis=dim, tiled=True)]
    pallas_call x0 -> x1, Pallas kernels: none -> 129 us  [shards(): pl.pallas_call(functools.partial(layer, groups, spans, peers), name='laye...]
    all_gather x6 -> x0, blocking collectives: 72.2 us -> none  [entering_2(): pieces = jax.tree.map(lambda part: lax.all_gather(part, axis), running)]
    all_to_all x2 -> x0, blocking collectives: 25 us -> none  [the longest x1 12.8 us: summed_on_arrival(): lax.all_to_all(parts, axis, split_axis=0, concat_axis=0, tiled=True)]
    dot_general x11 -> x0, matrix products: 17.6 us -> none  [the longest x1 5.98 us: shards(): jnp.dot(gathered_copies(normed, 'tp', 0), pair_full, preferred_element_ty...]
    unnamed x23 -> x27, local copies, waits for them, and re-layouts: 0.17 us -> 11.1 us
    all_to_all x1 -> x0, waiting for transfers between devices: 6.93 us -> none  [summed_on_arrival(): lax.all_to_all(parts, axis, split_axis=0, concat_axis=0, tiled=True)]
    ppermute x2 -> x0, starting transfers between devices: 4.38 us -> none  [the longest x1 2.43 us: padded_2(): after = lax.ppermute(initial, axis, down)]
  transfers between devices with their start and end apart: 6 -> 0, of which waited for: 5 -> 0; matrix products, arithmetic and copies ran while one was open for 4% -> 0% of each run, Pallas kernels for 0% -> 0%
where the time goes in v1:
time: 142 us; the launch traced here: 141 us
  Pallas kernels  129 us (91%)
  local copies, waits for them, and re-layouts  11.8 us (8%)
    pallas_call x1, Pallas kernels, shards(): pl.pallas_call(functools.partial(layer, groups, spans, peers), name='laye...  129 us
    unnamed x27, local copies, waits for them, and re-layouts  11.1 us

profile of v1, /device:TPU:33, one launch (start us, length us, event | category | flops | bytes accessed | tf_op | source)
XLA Modules:
  0.0 140.9 jit_solution(11111578217688705002)
XLA Ops:
  0.0 0.0 copy-start.9
  0.0 0.7 reshape.3.ng_ref
  0.7 0.0 copy-done.9
  0.7 0.0 copy-start
  0.7 1.2 copy-done
  1.9 0.0 copy-start.1
  1.9 1.0 copy-done.1
  3.0 0.0 copy-start.2
  3.0 0.9 copy-done.2
  3.9 0.0 copy-start.3
  3.9 0.9 copy-done.3
  4.8 0.0 copy-start.4
  4.8 0.9 copy-done.4
  5.8 0.0 copy-start.5
  5.8 0.8 copy-done.5
  6.6 0.0 copy-start.6
  6.6 0.8 copy-done.6
  7.4 0.0 copy-start.7
  7.4 0.8 copy-done.7
  8.3 0.0 copy-start.8
  8.3 0.8 copy-done.8
  9.1 0.0 copy-start.10
  9.1 0.7 copy-done.10
  9.8 0.0 copy-start.11
  9.8 0.7 copy-done.11
  10.5 0.0 copy-start.12
  10.5 0.7 copy-done.12
  11.2 129.1 %layer.1 = bf16[32,2048]{1,0:T(8,128)(2,1)S(1)} custom-call(bf16[128,256]{1,0:T(8,128)(2,1)S(1)} %copy-done.5, bf16[128,256]{1,0:T(8,128)(2,1)S(1)} %copy-done.6, bf16[128,256]{1,0:T(8,128)(2,1)S(1)} %copy-done.7, bf16[128,256]{1,0:T(8,128)(2,1)S(1)} %copy-done.8, f32[2,2,128]{2,1,0:T(2,128)S(1)} %copy-done.11, f32[2,256]{1,0:T(2,128)S(1)} %copy-done.12, ...), custom_call_target="tpu_custom_call" | custom-call | tf_op jit(solution)/shard_map/layer/pallas_call | solution.py:551
  140.3 0.7 copy.16
Async XLA Ops:
  0.0 0.7 copy-start.9
  0.7 1.2 copy-start
  1.9 1.0 copy-start.1
  3.0 0.9 copy-start.2
  3.9 0.9 copy-start.3
  4.8 0.9 copy-start.4
  5.8 0.8 copy-start.5
  6.6 0.8 copy-start.6
  7.4 0.8 copy-start.7
  8.3 0.8 copy-start.8
  9.1 0.7 copy-start.10
  9.8 0.7 copy-start.11
  10.5 0.7 copy-start.12

commit v2 on v1

--- a/solution.py
+++ b/solution.py
@@ -35,7 +35,7 @@
         self.tp = lax.axis_index("tp")
         self.core = lax.rem(self.sp, 2)
         self.z = lax.div(self.sp, 2)
-        self.paired = groups % 2 == 0
+        self.paired = PAIRED and groups % 2 == 0
         grp = lax.axis_index("grp")
         self.side = lax.rem(grp, 2)
         self.pair = {"grp": grp + 1 - 2 * self.side}
@@ -70,7 +70,7 @@
         self.ring_s, self.ring_r, self.pair_s, self.pair_r, self.twin_s, self.twin_r, self.twin2_s, self.twin2_r = sems
         width = buf.shape[1]
         tiles = width // LANE
-        ring = round(2 * tiles / 3) if place.paired else tiles
+        ring = max((tiles + 1) // 2, int(RING_SHARE * tiles)) if place.paired else tiles
         self.width = width
         self.ring_w = ring * LANE
         self.pair_w = width - self.ring_w
@@ -177,45 +177,42 @@
             copy.wait_send()
 
 
-def order(gate_up, down, last, lag):
+def order(gate_up, down, last):
     late = []
 
     def one(stream, step, half):
+        while len(late) > PAIR_LAG:
+            a, b, c = late.pop(0)
+            a.pair_tick(b, c)
         stream.tick(step, half)
         late.append((stream, step, half))
 
-    for step in range(1, last + lag + 1):
+    for step in range(1, last + DOWN_LAG + 1):
         for half in range(gate_up.halves):
             if step <= last:
-                while len(late) > 1:
-                    a, b, c = late.pop(0)
-                    a.pair_tick(b, c)
                 one(gate_up, step, half)
                 yield
         for half in range(down.halves):
-            if step == lag:
+            if step == DOWN_LAG:
                 down.own(half)
-            elif step > lag:
-                while len(late) > 1:
-                    a, b, c = late.pop(0)
-                    a.pair_tick(b, c)
-                one(down, step - lag, half)
+            elif step > DOWN_LAG:
+                one(down, step - DOWN_LAG, half)
                 yield
     for a, b, c in late:
         a.pair_tick(b, c)
 
 
 def all_to_all(place, src, dst, send_sem, recv_sem):
-    spans = place.spans
+    chips = place.chips
 
     def body(t, _):
-        step = spans // 2 + (1 - 2 * lax.rem(t, 2)) * lax.div(t + 1, 2)
-        to = lax.rem(place.sp + step, spans)
-        for s, d, ss, rs in zip(src(to), dst(place.sp), send_sem, recv_sem):
-            remote(s, d, ss, rs, {"sp": to}).start()
+        step = chips // 2 + (1 - 2 * lax.rem(t, 2)) * lax.div(t + 1, 2)
+        to = lax.rem(place.z + step, chips)
+        for s, d, ss, rs in zip(src(to), dst(place.z), send_sem, recv_sem):
+            remote(s, d, ss, rs, {"sp": 2 * to + place.core}).start()
         return 0
 
-    lax.fori_loop(0, spans - 1, body, 0)
+    lax.fori_loop(0, chips - 1, body, 0)
 
 
 def wait_bytes(view, sem):
@@ -224,17 +221,17 @@
 
 def layer(
     groups, spans, peers,
-    q_ref, k_ref, v_ref, g_ref, ld_ref, hg_ref, wo_hbm, res_hbm, ng_ref, gw_hbm, uw_hbm, dw_hbm, gt_ref, ut_ref,
+    q_hbm, k_hbm, v_hbm, g_hbm, ld_hbm, hg_hbm, wo_hbm, res_hbm, ng_hbm, gw_hbm, uw_hbm, dw_hbm, gt_hbm, ut_hbm,
     out_ref,
-    gu, dn, wo, res, st_send, st_recv, dec_send, dec_recv, in_send, in_recv, inner, grow, mix, att, att_r,
+    q_ref, k_ref, v_ref, g_ref, ld_ref, hg_ref, ng_ref, gt_ref, ut_ref, gu, dn, wo, res, st, st_twin, dec, dec_twin, st_send, st_recv, dec_send, dec_recv, in_send, in_recv, in_twin, inner, grow, mix, att, att_r,
     mid, nsend, nall, nperm, pre, halo_s, halo_r, hid, ff, ff_r,
-    load_sem, a2a_s, a2a_r, rs1_s, rs1_r, ag_s, ag_r, halo_ss, halo_rs, rs2_s, rs2_r,
+    load_sem, twin_s, twin_r, a2a_s, a2a_r, rs1_s, rs1_r, ag_s, ag_r, halo_ss, halo_rs, rs2_s, rs2_r,
     g0, g1, g2, g3, g4, g5, g6, g7, d0, d1, d2, d3, d4, d5, d6, d7,
 ):
     place = Place(groups, spans, peers)
     sp, tp, core = place.sp, place.tp, place.core
-    length = q_ref.shape[0]
-    heads = q_ref.shape[1] // HEAD
+    length = q_hbm.shape[0]
+    heads = q_hbm.shape[1] // HEAD
     combos = 2 * heads
     share = length // peers
     half_w = gw_hbm.shape[1]
@@ -242,36 +239,35 @@
     slots = place.chips
     scale = HEAD ** (-0.5)
 
+    own_rows = pl.ds(pl.multiple_of(core * block, block), block)
+    pairs = [
+        (q_hbm, q_ref), (k_hbm, k_ref), (v_hbm, v_ref), (ld_hbm, ld_ref),
+        (gw_hbm, gu.at[own_rows, pl.ds(0, half_w)]), (uw_hbm, gu.at[own_rows, pl.ds(half_w, half_w)]),
+        (dw_hbm, dn.at[own_rows, :]), (g_hbm, g_ref), (hg_hbm, hg_ref), (wo_hbm, wo),
+        (res_hbm.at[pl.ds(pl.multiple_of(tp * share, share), share), :], res), (ng_hbm, ng_ref), (gt_hbm, gt_ref),
+        (ut_hbm, ut_ref),
+    ]
+    loads = [pltpu.make_async_copy(src, dst, load_sem.at[n]) for n, (src, dst) in enumerate(pairs)]
+    for copy in loads:
+        copy.start()
+
     barrier = pltpu.get_barrier_semaphore()
 
     def greet(step, _):
-        pl.semaphore_signal(barrier, inc=1, device_id={"sp": place.span(step)}, device_id_type=MESH)
+        pl.semaphore_signal(barrier, inc=1, device_id=place.along(step), device_id_type=MESH)
         return 0
 
-    pl.semaphore_signal(barrier, inc=1, device_id=place.along(1), device_id_type=MESH)
-    pl.semaphore_signal(barrier, inc=1, device_id=place.along(-1), device_id_type=MESH)
-    lax.fori_loop(3, spans - 2, greet, 0)
-    for step in (1, 2 * 0 + spans - 1):
-        pl.semaphore_signal(barrier, inc=1, device_id={"sp": place.span(step)}, device_id_type=MESH)
-    greeted = spans - 1
-    for step in range(1, peers):
-        pl.semaphore_signal(barrier, inc=1, device_id={"tp": place.peer(step)}, device_id_type=MESH)
-    greeted += peers - 1
+    lax.fori_loop(1, place.chips, greet, 0)
+    beside = {"sp": place.span(2 * core - 1)}
+    for device in [place.twin, beside] + [{"tp": place.peer(step)} for step in range(1, peers)]:
+        pl.semaphore_signal(barrier, inc=1, device_id=device, device_id_type=MESH)
+    greeted = place.chips + peers
     if place.paired:
         pl.semaphore_signal(barrier, inc=1, device_id=place.pair, device_id_type=MESH)
         greeted += 1
 
-    own_rows = pl.ds(pl.multiple_of(core * block, block), block)
-    loads = [
-        pltpu.make_async_copy(gw_hbm, gu.at[own_rows, pl.ds(0, half_w)], load_sem.at[0]),
-        pltpu.make_async_copy(uw_hbm, gu.at[own_rows, pl.ds(half_w, half_w)], load_sem.at[1]),
-        pltpu.make_async_copy(dw_hbm, dn.at[own_rows, :], load_sem.at[2]),
-        pltpu.make_async_copy(wo_hbm, wo, load_sem.at[3]),
-        pltpu.make_async_copy(res_hbm.at[pl.ds(pl.multiple_of(tp * share, share), share), :], res, load_sem.at[4]),
-    ]
-    for copy in loads:
-        copy.start()
-
+    for copy in loads[:4]:
+        copy.wait()
     row = lax.broadcasted_iota(jnp.int32, (HEAD, LANE), 0)
     lane = lax.broadcasted_iota(jnp.int32, (HEAD, LANE), 1)
     rates = [ld_ref[d, pl.ds(h, 1), :] for h in range(heads) for d in range(2)]
@@ -285,7 +281,8 @@
         bwd = jnp.where(s_lane < length - shift, pltpu.roll(sums, length - shift, 1), 0.0)
         sums = sums + jnp.where(back, bwd, fwd)
         shift *= 2
-    part = spans // combos
+    chips = place.chips
+    part = chips // 2
     rows = HEAD // part
     for h in range(heads):
         cols = pl.ds(h * HEAD, HEAD)
@@ -301,13 +298,13 @@
             inner[m] = nn((scores * decay).astype(BF16), v)
             grow[m] = jnp.exp(along_t) * scale
             total = along_t[length - 1 : length, :] if d == 0 else along_t[0:1, :]
-            dec_send[m] = jnp.exp(total)
+            dec[m] = jnp.exp(total)
             faded = (v32 * jnp.exp(jnp.minimum(total - along_t, 0.0))).astype(BF16)
-            st_send[pl.ds(m * part, part)] = tn(k, faded).astype(BF16).reshape(part, rows, HEAD)
-
-    gate_up = Stream(place, gu, 2, (g0, g1, g2, g3, g4, g5, g6, g7))
-    down = Stream(place, dn, 2, (d0, d1, d2, d3, d4, d5, d6, d7))
-    ring = order(gate_up, down, place.chips // 2, 2)
+            st[m] = tn(k, faded).astype(BF16)
+
+    gate_up = Stream(place, gu, GU_PARTS, (g0, g1, g2, g3, g4, g5, g6, g7))
+    down = Stream(place, dn, DOWN_PARTS, (d0, d1, d2, d3, d4, d5, d6, d7))
+    ring = order(gate_up, down, place.chips // 2)
 
     def advance(n):
         for _ in range(n):
@@ -319,10 +316,29 @@
                 next(ring, None)
             stream.ready(slot)
 
-    for copy in loads[:3]:
+    for copy in loads[4:7]:
         copy.wait()
     pl.semaphore_wait(barrier, greeted)
 
+    swaps = [
+        remote(st, st_twin, twin_s.at[0], twin_r.at[0], place.twin),
+        remote(dec, dec_twin, twin_s.at[1], twin_r.at[1], place.twin),
+    ]
+    for copy in swaps:
+        copy.start()
+    for part_no in range(OWN_FIRST):
+        gate_up.own(part_no)
+    for copy in swaps:
+        copy.wait_recv()
+    second = (core == 1).astype(F32)
+    for d in range(2):
+        m = 2 * core + d
+        far = second if d == 0 else 1.0 - second
+        mine, other = st[m].astype(F32), st_twin[m].astype(F32)
+        my_dec, other_dec = dec[m], dec_twin[m]
+        merged = mine * (far + (1.0 - far) * other_dec) + other * ((1.0 - far) + far * my_dec)
+        st_send[pl.ds(d * part, part)] = merged.astype(BF16).reshape(part, rows, HEAD)
+        dec_send[d] = my_dec * other_dec
     all_to_all(
         place,
         lambda to: (st_send.at[to], dec_send.at[lax.div(to, part)]),
@@ -330,32 +346,34 @@
         (a2a_s.at[0], a2a_s.at[1]),
         (a2a_r.at[0], a2a_r.at[1]),
     )
-    gate_up.own(0)
-    gate_up.own(1)
-    my_combo = lax.div(sp, part)
-    st_recv[pl.ds(sp, 1)] = st_send[pl.ds(sp, 1)]
-    dec_recv[pl.ds(sp, 1)] = dec_send[pl.ds(my_combo, 1)]
+    for part_no in range(OWN_FIRST, GU_PARTS):
+        gate_up.own(part_no)
+    reverse = lax.div(place.z, part)
+    st_recv[pl.ds(place.z, 1)] = st_send[pl.ds(place.z, 1)]
+    dec_recv[pl.ds(place.z, 1)] = dec_send[pl.ds(reverse, 1)]
     advance(ADVANCE[0])
-    others = pl.ds(0, spans - 1)
+    others = pl.ds(0, chips - 1)
     wait_bytes(st_recv.at[others], a2a_r.at[0])
     wait_bytes(dec_recv.at[others], a2a_r.at[1])
 
-    reverse = lax.rem(my_combo, 2)
-
     def scan(j, carry):
-        at = j + reverse * (spans - 1 - 2 * j)
+        at = j + reverse * (chips - 1 - 2 * j)
         in_send[at] = carry.astype(BF16)
         return carry * dec_recv[at] + st_recv[at].astype(F32)
 
-    lax.fori_loop(0, spans, scan, jnp.zeros((rows, HEAD), F32))
+    lax.fori_loop(0, chips, scan, jnp.zeros((rows, HEAD), F32))
     all_to_all(
-        place, lambda to: (in_send.at[to],), lambda me: (in_recv.at[me],), (a2a_s.at[2],), (a2a_r.at[2],)
+        place, lambda to: (in_send.at[to],), lambda me: (in_recv.at[core, me],), (a2a_s.at[2],), (a2a_r.at[2],)
     )
-    in_recv[pl.ds(sp, 1)] = in_send[pl.ds(sp, 1)]
+    in_recv[core, pl.ds(place.z, 1)] = in_send[pl.ds(place.z, 1)]
     advance(ADVANCE[1])
-    for copy in loads[3:]:
+    wait_bytes(in_recv.at[core, others], a2a_r.at[2])
+    handover = remote(in_recv.at[core], in_twin, twin_s.at[2], twin_r.at[2], place.twin)
+    handover.start()
+    for copy in loads[7:]:
         copy.wait()
-    wait_bytes(in_recv.at[others], a2a_r.at[2])
+    handover.wait_recv()
+    in_recv[1 - core] = in_twin[...]
 
     def normed_head(x):
         centre = x - jnp.mean(x, axis=1, keepdims=True)
@@ -368,7 +386,10 @@
         combined = None
         for d in range(2):
             m = 2 * h + d
-            state = in_recv[pl.ds(m * part, part)].reshape(HEAD, HEAD)
+            state = in_recv[h, pl.ds(d * part, part)].reshape(HEAD, HEAD).astype(F32)
+            far = second if d == 0 else 1.0 - second
+            state = state * (far * dec_twin[m] + (1.0 - far)) + far * st_twin[m].astype(F32)
+            state = state.astype(BF16)
             term = normed_head(inner[m] + grow[m] * nn(q, state)) * hg_ref[pl.ds(d, 1), cols]
             combined = term if combined is None else combined + term
         gate = g_ref[:, cols].astype(F32)
@@ -402,7 +423,7 @@
     mid[...] = middle
     values = middle.astype(F32)
     multiplier = lax.rsqrt(jnp.mean(values * values, axis=1, keepdims=True) + NORM_EPS)
-    normed = (values * multiplier * ng_ref[...].astype(F32)).astype(BF16)
+    normed = (values * multiplier * ng_ref[...].astype(F32).reshape(1, -1)).astype(BF16)
     nsend[...] = normed
     nall[peer_rows(tp), :] = normed
     to_peers(lambda j: nsend, lambda step: nall.at[peer_rows(tp), :], ag_s, ag_r)
@@ -415,16 +436,27 @@
         nperm[:, pl.ds(slot * LANE, LANE)] = nall[:, pl.ds(start, LANE)]
 
     advance(ADVANCE[4])
-    ready(gate_up, 0, slots)
-
+    early = slots - 3
+    ready(gate_up, 0, early)
     n_tile = 256 if (2 * half_w) % 256 == 0 else 128
+    head_k, tail_k = pl.ds(0, early * 2 * block), pl.ds(early * 2 * block, (slots - early) * 2 * block)
+
+    def tile_cols(n):
+        return pl.ds(pl.multiple_of(n * n_tile, n_tile), n_tile)
 
     def project(n, _):
-        cols = pl.ds(pl.multiple_of(n * n_tile, n_tile), n_tile)
-        pre[:, cols] = nn(nperm[...], gu[:, cols]).astype(BF16).astype(F32)
+        pre[:, tile_cols(n)] = nn(nperm[:, head_k], gu[head_k, tile_cols(n)])
         return 0
 
     lax.fori_loop(0, 2 * half_w // n_tile, project, 0)
+    ready(gate_up, early, slots)
+
+    def project_rest(n, _):
+        total = pre[:, tile_cols(n)] + nn(nperm[:, tail_k], gu[tail_k, tile_cols(n)])
+        pre[:, tile_cols(n)] = total.astype(BF16).astype(F32)
+        return 0
+
+    lax.fori_loop(0, 2 * half_w // n_tile, project_rest, 0)
     halo_s[0] = pre[0:1, :]
     halo_s[1] = pre[length - 1 : length, :]
     before, after = {"sp": place.span(-1)}, {"sp": place.span(1)}
@@ -455,8 +487,9 @@
 
     lax.fori_loop(0, half_w // LANE, conv, 0)
 
-    cut = slots // 2
-    for part_no, (lo, hi) in enumerate(((0, cut), (cut, slots))):
+    cuts = sorted({0, slots // 2, slots - 2, slots})
+    pieces = list(zip(cuts[:-1], cuts[1:]))
+    for part_no, (lo, hi) in enumerate(pieces):
         ready(down, lo, hi)
 
         def project_down(n, _):
@@ -472,7 +505,7 @@
             rs2_s.at[part_no],
             rs2_r.at[part_no],
         )
-    for part_no, (lo, hi) in enumerate(((0, cut), (cut, slots))):
+    for part_no, (lo, hi) in enumerate(pieces):
         cols = pl.ds(lo * LANE, (hi - lo) * LANE)
         for step in range(1, peers):
             view = ff_r.at[step - 1, :, cols]
@@ -488,6 +521,8 @@
     advance(10_000)
     for copy in started + halos:
         copy.wait_send()
+    for copy in swaps + [handover]:
+        copy.wait_send()
     wait_bytes(st_send.at[others], a2a_s.at[0])
     wait_bytes(dec_recv.at[others], a2a_s.at[1])
     wait_bytes(in_send.at[others], a2a_s.at[2])
@@ -495,7 +530,14 @@
     down.drain()
 
 
-ADVANCE = (3, 3, 4, 5, 10, 3)
+PAIRED = True
+OWN_FIRST = 1
+RING_SHARE = 0.66
+PAIR_LAG = 2
+DOWN_LAG = 1
+GU_PARTS = 2
+DOWN_PARTS = 2
+ADVANCE = (4, 7, 4, 4, 0, 2)
 
 
 def solution(mesh):
@@ -515,21 +557,26 @@
         block, half_w = gw.shape
         width = wo.shape[1]
         chips = spans // 2
-        packet = HEAD * combos // spans
+        packet = 2 * HEAD // chips
         dma = pltpu.SemaphoreType.DMA
         vmem = pl.BlockSpec(memory_space=pltpu.VMEM)
-        any_ = pl.BlockSpec(memory_space=pl.ANY)
-        scratch = [
+        hbm = pl.BlockSpec(memory_space=pltpu.HBM)
+        scratch = [pltpu.VMEM(a.shape, a.dtype) for a in (q, k, v, g, ld, hg, ng, gt, ut)] + [
             pltpu.VMEM((spans * block, 2 * half_w), BF16),
             pltpu.VMEM((spans * block, half_w), BF16),
             pltpu.VMEM(wo.shape, BF16),
             pltpu.VMEM((share, width), BF16),
-            pltpu.VMEM((spans, packet, HEAD), BF16),
-            pltpu.VMEM((spans, packet, HEAD), BF16),
+            pltpu.VMEM((combos, HEAD, HEAD), BF16),
+            pltpu.VMEM((combos, HEAD, HEAD), BF16),
             pltpu.VMEM((combos, 1, LANE), F32),
-            pltpu.VMEM((spans, 1, LANE), F32),
-            pltpu.VMEM((spans, packet, HEAD), BF16),
-            pltpu.VMEM((spans, packet, HEAD), BF16),
+            pltpu.VMEM((combos, 1, LANE), F32),
+            pltpu.VMEM((chips, packet, HEAD), BF16),
+            pltpu.VMEM((chips, packet, HEAD), BF16),
+            pltpu.VMEM((2, 1, LANE), F32),
+            pltpu.VMEM((chips, 1, LANE), F32),
+            pltpu.VMEM((chips, packet, HEAD), BF16),
+            pltpu.VMEM((2, chips, packet, HEAD), BF16),
+            pltpu.VMEM((chips, packet, HEAD), BF16),
             pltpu.VMEM((combos, length, HEAD), F32),
             pltpu.VMEM((combos, length, HEAD), F32),
             pltpu.VMEM((length, heads * HEAD), BF16),
@@ -545,19 +592,19 @@
             pltpu.VMEM((length, half_w), BF16),
             pltpu.VMEM((length, width), BF16),
             pltpu.VMEM((peers - 1, share, width), BF16),
-            dma((5,)), dma((3,)), dma((3,)), dma((peers - 1,)), dma((peers - 1,)), dma((peers - 1,)), dma((peers - 1,)),
-            dma((2,)), dma((2,)), dma((2, peers - 1)), dma((2, peers - 1)),
-        ] + [dma((chips, 2)) for _ in range(16)]
+            dma((14,)), dma((3,)), dma((3,)), dma((3,)), dma((3,)), dma((peers - 1,)), dma((peers - 1,)), dma((peers - 1,)), dma((peers - 1,)),
+            dma((2,)), dma((2,)), dma((3, peers - 1)), dma((3, peers - 1)),
+        ] + [dma((chips, n)) for n in (GU_PARTS, DOWN_PARTS) for _ in range(8)]
         return pl.pallas_call(
             functools.partial(layer, groups, spans, peers),
             name="layer",
             out_shape=jax.ShapeDtypeStruct((share, width), BF16),
-            in_specs=[vmem] * 6 + [any_, any_, vmem, any_, any_, any_, vmem, vmem],
+            in_specs=[hbm] * 14,
             out_specs=vmem,
             scratch_shapes=scratch,
             compiler_params=pltpu.CompilerParams(
-                collective_id=0, has_side_effects=True, vmem_limit_bytes=50 * 1024 * 1024
+                collective_id=0, has_side_effects=True, vmem_limit_bytes=67_043_328
             ),
-        )(q, k, v, g, ld, hg, wo, res, ng.reshape(1, -1), gw, uw, dw, gt, ut)
+        )(q, k, v, g, ld, hg, wo, res, ng, gw, uw, dw, gt, ut)
 
     return jax.shard_map(shards, mesh=mesh, in_specs=placed, out_specs=P(("grp", "sp", "tp"), None), check_vma=False)

time: 142 us -> 121 us (0.85)
  local copies, waits for them, and re-layouts: 11.8 us -> 1.57 us
  Pallas kernels: 129 us -> 120 us
    pallas_call x1, Pallas kernels: 129 us -> 120 us  [shards(): pl.pallas_call(functools.partial(layer, groups, spans, peers), name='laye...]
    unnamed x27 -> x1, local copies, waits for them, and re-layouts: 11.1 us -> 1.57 us
where the time goes in v2:
time: 121 us
  Pallas kernels  120 us (99%)
  local copies, waits for them, and re-layouts  1.57 us (1%)
    pallas_call x1, Pallas kernels, shards(): pl.pallas_call(functools.partial(layer, groups, spans, peers), name='laye...  120 us

profile of v2, /device:TPU:33, one launch (start us, length us, event | category | flops | bytes accessed | tf_op | source)
XLA Modules:
  0.0 121.1 jit_solution(16345875892476902129)
XLA Ops:
  0.0 119.5 %layer.1 = bf16[32,2048]{1,0:T(8,128)(2,1)} custom-call(bf16[128,256]{1,0:T(8,128)(2,1)} %q_hbm.1, bf16[128,256]{1,0:T(8,128)(2,1)} %k_hbm.1, bf16[128,256]{1,0:T(8,128)(2,1)} %v_hbm.1, bf16[128,256]{1,0:T(8,128)(2,1)} %g_hbm.1, f32[2,2,128]{2,1,0:T(2,128)} %ld_hbm.1, f32[2,256]{1,0:T(2,128)} %hg_hbm.1, bf16[256,2048]{1,0:T(8,128)(2,1)} %wo_hbm.1, ...), custom_call_target="tpu_custom_call" | custom-call | tf_op jit(solution)/shard_map/layer/pallas_call | solution.py:598
  119.5 1.6 %copy.16 = bf16[32,2048]{1,0:T(8,128)(2,1)} copy(bf16[32,2048]{1,0:T(8,128)(2,1)} %layer.1) | data formatting | bytes 262144

commit v3 on v2

--- a/solution.py
+++ b/solution.py
@@ -26,6 +26,12 @@
 
 def nn(a, b):
     return jnp.dot(a, b, preferred_element_type=F32)
+
+
+def groups_of(slots):
+    early = slots - EARLY
+    cuts = sorted({0, slots // 2, slots - 2, slots})
+    return [(0, early), (early, slots)], list(zip(cuts[:-1], cuts[1:]))
 
 
 class Place:
@@ -65,12 +71,13 @@
 
 
 class Stream:
-    def __init__(self, place, buf, halves, sems):
-        self.p, self.buf, self.halves = place, buf, halves
-        self.ring_s, self.ring_r, self.pair_s, self.pair_r, self.twin_s, self.twin_r, self.twin2_s, self.twin2_r = sems
+    def __init__(self, place, buf, share, parts, groups, send_s, ring_r, pair_r, twin_r):
+        self.p, self.buf, self.parts, self.groups = place, buf, parts, groups
+        self.ring_s, self.pair_s, self.twin_s = (send_s.at[n] for n in range(3))
+        self.ring_r, self.pair_r, self.twin_r = ring_r, pair_r, twin_r
         width = buf.shape[1]
         tiles = width // LANE
-        ring = max((tiles + 1) // 2, int(RING_SHARE * tiles)) if place.paired else tiles
+        ring = max((tiles + 1) // 2, int(share * tiles)) if place.paired else tiles
         self.width = width
         self.ring_w = ring * LANE
         self.pair_w = width - self.ring_w
@@ -78,125 +85,106 @@
         self.pair_o = pl.multiple_of((1 - place.side) * self.ring_w, LANE)
         self.give_o = pl.multiple_of(place.side * self.ring_w, LANE)
         self.block = buf.shape[0] // place.spans
-        self.rows = self.block // halves
+        self.rows = self.block // parts
         self.last = place.chips // 2
         self.opposite = place.chips - 1
-        self.started = []
         self.handed = {0}
 
-    def view(self, slot, half, cols, core=None):
-        core = self.p.core if core is None else core
-        start = pl.multiple_of(slot * 2 * self.block + core * self.block + half * self.rows, self.rows)
+    def view(self, slot, part, cols):
+        start = pl.multiple_of(slot * 2 * self.block + self.p.core * self.block + part * self.rows, self.rows)
         return self.buf.at[pl.ds(start, self.rows), cols]
+
+    def bulk(self, rows, width):
+        return self.buf.at[pl.ds(0, rows), pl.ds(0, width)]
 
     def ring_cols(self):
         return pl.ds(self.ring_o, self.ring_w)
 
-    def send(self, src, dst, s, r, device):
-        copy = remote(src, dst, s, r, device)
-        copy.start()
-        self.started.append(copy)
-
-    def to_twin(self, slot, half, cols, s, r):
-        view = self.view(slot, half, cols)
-        self.send(view, view, s.at[slot, half], r.at[slot, half], self.p.twin)
-
-    def to_pair(self, slot, half):
-        if self.p.paired:
-            view = self.view(slot, half, pl.ds(self.give_o, self.pair_w))
-            self.send(view, view, self.pair_s.at[slot, half], self.pair_r.at[slot, half], self.p.pair)
-
-    def own(self, half):
+    def slots(self, step):
+        return (self.opposite,) if step == self.last else (2 * step - 1, 2 * step)
+
+    def on(self, src_slot, dst_slot, part, way):
         cols = self.ring_cols()
-        src = self.view(0, half, cols)
-        self.send(src, self.view(1, half, cols), self.ring_s.at[0, half], self.ring_r.at[1, half], self.p.along(1))
-        self.send(
-            src, self.view(2, half, cols), self.ring_s.at[self.opposite, half], self.ring_r.at[2, half], self.p.along(-1)
-        )
-        self.to_twin(0, half, pl.ds(0, self.width), self.twin_s, self.twin_r)
-
-    def got(self, slot, half):
-        view = self.view(slot, half, self.ring_cols())
-        remote(view, view, self.ring_s.at[slot, half], self.ring_r.at[slot, half], self.p.along(1)).wait_recv()
-
-    def tick(self, step, half):
-        cols = self.ring_cols()
+        src, dst = self.view(src_slot, part, cols), self.view(dst_slot, part, cols)
+        remote(src, dst, self.ring_s, self.ring_r.at[dst_slot, part], self.p.along(way)).start()
+
+    def to_twin(self, slot, part, cols):
+        view = self.view(slot, part, cols)
+        group = [n for n, (lo, hi) in enumerate(self.groups) if lo <= slot < hi][0]
+        remote(view, view, self.twin_s, self.twin_r.at[group], self.p.twin).start()
+
+    def own(self, part):
+        self.on(0, 1, part, 1)
+        self.on(0, 2, part, -1)
+        self.to_twin(0, part, pl.ds(0, self.width))
+
+    def got(self, slot, part):
+        view = self.view(slot, part, self.ring_cols())
+        wait_bytes(view, self.ring_r.at[slot, part])
+
+    def tick(self, step, part):
         if step == self.last:
-            slots = (self.opposite,)
-            self.got(self.opposite, half)
+            self.got(self.opposite, part)
         else:
-            behind, ahead = slots = (2 * step - 1, 2 * step)
+            behind, ahead = self.slots(step)
             if step + 1 < self.last:
-                for slot, way in ((behind, 1), (ahead, -1)):
-                    self.got(slot, half)
-                    self.send(
-                        self.view(slot, half, cols),
-                        self.view(slot + 2, half, cols),
-                        self.ring_s.at[slot, half],
-                        self.ring_r.at[slot + 2, half],
-                        self.p.along(way),
-                    )
+                self.got(behind, part)
+                self.on(behind, behind + 2, part, 1)
+                self.got(ahead, part)
+                self.on(ahead, ahead + 2, part, -1)
             else:
-                self.got(behind, half)
-                self.got(ahead, half)
-                slot = behind + self.p.core
-                self.send(
-                    self.view(slot, half, cols),
-                    self.view(self.opposite, half, cols),
-                    self.ring_s.at[slot, half],
-                    self.ring_r.at[self.opposite, half],
-                    self.p.along(1 - 2 * self.p.core),
-                )
-        for slot in slots:
-            self.to_pair(slot, half)
-            self.to_twin(slot, half, cols, self.twin_s, self.twin_r)
-
-    def pair_tick(self, step, half):
-        slots = (self.opposite,) if step == self.last else (2 * step - 1, 2 * step)
-        if half == self.halves - 1:
+                self.got(behind, part)
+                self.got(ahead, part)
+                self.on(behind + self.p.core, self.opposite, part, 1 - 2 * self.p.core)
+        for slot in self.slots(step):
+            if self.p.paired:
+                view = self.view(slot, part, pl.ds(self.give_o, self.pair_w))
+                remote(view, view, self.pair_s, self.pair_r.at[step, part], self.p.pair).start()
+        for slot in self.slots(step):
+            self.to_twin(slot, part, self.ring_cols())
+
+    def pair_tick(self, step, part):
+        slots = self.slots(step)
+        if part == self.parts - 1:
             self.handed.update(slots)
         if not self.p.paired:
             return
-        cols = pl.ds(self.pair_o, self.pair_w)
+        wait_bytes(self.bulk(len(slots) * self.rows, self.pair_w), self.pair_r.at[step, part])
         for slot in slots:
-            view = self.view(slot, half, cols)
-            remote(view, view, self.pair_s.at[slot, half], self.pair_r.at[slot, half], self.p.pair).wait_recv()
-            self.to_twin(slot, half, cols, self.twin2_s, self.twin2_r)
-
-    def ready(self, slot):
-        for half in range(self.halves):
-            cols = pl.ds(0, self.width) if slot == 0 else self.ring_cols()
-            view = self.view(slot, half, cols, 1 - self.p.core)
-            remote(view, view, self.twin_s.at[slot, half], self.twin_r.at[slot, half], self.p.twin).wait_recv()
-            if self.p.paired and slot > 0:
-                view = self.view(slot, half, pl.ds(self.pair_o, self.pair_w), 1 - self.p.core)
-                remote(view, view, self.twin2_s.at[slot, half], self.twin2_r.at[slot, half], self.p.twin).wait_recv()
+            self.to_twin(slot, part, pl.ds(self.pair_o, self.pair_w))
+
+    def ready(self, group):
+        lo, hi = self.groups[group]
+        wait_bytes(self.bulk((hi - lo) * self.block, self.width), self.twin_r.at[group])
 
     def drain(self):
-        for copy in self.started:
-            copy.wait_send()
+        rest = (self.p.chips - 1) * self.block
+        wait_bytes(self.bulk(rest, self.ring_w), self.ring_s)
+        if self.p.paired:
+            wait_bytes(self.bulk(rest, self.pair_w), self.pair_s)
+        wait_bytes(self.bulk(rest + self.block, self.width), self.twin_s)
 
 
 def order(gate_up, down, last):
     late = []
 
-    def one(stream, step, half):
+    def one(stream, step, part):
         while len(late) > PAIR_LAG:
             a, b, c = late.pop(0)
             a.pair_tick(b, c)
-        stream.tick(step, half)
-        late.append((stream, step, half))
+        stream.tick(step, part)
+        late.append((stream, step, part))
 
     for step in range(1, last + DOWN_LAG + 1):
-        for half in range(gate_up.halves):
+        for part in range(gate_up.parts):
             if step <= last:
-                one(gate_up, step, half)
+                one(gate_up, step, part)
                 yield
-        for half in range(down.halves):
+        for part in range(down.parts):
             if step == DOWN_LAG:
-                down.own(half)
+                down.own(part)
             elif step > DOWN_LAG:
-                one(down, step - DOWN_LAG, half)
+                one(down, step - DOWN_LAG, part)
                 yield
     for a, b, c in late:
         a.pair_tick(b, c)
@@ -225,8 +213,8 @@
     out_ref,
     q_ref, k_ref, v_ref, g_ref, ld_ref, hg_ref, ng_ref, gt_ref, ut_ref, gu, dn, wo, res, st, st_twin, dec, dec_twin, st_send, st_recv, dec_send, dec_recv, in_send, in_recv, in_twin, inner, grow, mix, att, att_r,
     mid, nsend, nall, nperm, pre, halo_s, halo_r, hid, ff, ff_r,
-    load_sem, twin_s, twin_r, a2a_s, a2a_r, rs1_s, rs1_r, ag_s, ag_r, halo_ss, halo_rs, rs2_s, rs2_r,
-    g0, g1, g2, g3, g4, g5, g6, g7, d0, d1, d2, d3, d4, d5, d6, d7,
+    load_sem, twin_s, twin_r, a2a_s, a2a_r, tp_s, tp_r, halo_ss, halo_rs,
+    gu_s, gu_ring, gu_pair, gu_twin, dn_s, dn_ring, dn_pair, dn_twin,
 ):
     place = Place(groups, spans, peers)
     sp, tp, core = place.sp, place.tp, place.core
@@ -302,19 +290,19 @@
             faded = (v32 * jnp.exp(jnp.minimum(total - along_t, 0.0))).astype(BF16)
             st[m] = tn(k, faded).astype(BF16)
 
-    gate_up = Stream(place, gu, GU_PARTS, (g0, g1, g2, g3, g4, g5, g6, g7))
-    down = Stream(place, dn, DOWN_PARTS, (d0, d1, d2, d3, d4, d5, d6, d7))
+    early, cuts = groups_of(slots)
+    gate_up = Stream(place, gu, GU_SHARE, GU_PARTS, early, gu_s, gu_ring, gu_pair, gu_twin)
+    down = Stream(place, dn, DOWN_SHARE, DOWN_PARTS, cuts, dn_s, dn_ring, dn_pair, dn_twin)
     ring = order(gate_up, down, place.chips // 2)
 
     def advance(n):
         for _ in range(n):
             next(ring, None)
 
-    def ready(stream, first, end):
-        for slot in range(first, end):
-            while slot not in stream.handed:
-                next(ring, None)
-            stream.ready(slot)
+    def ready(stream, group):
+        while not stream.handed.issuperset(range(*stream.groups[group])):
+            next(ring, None)
+        stream.ready(group)
 
     for copy in loads[4:7]:
         copy.wait()
@@ -372,6 +360,7 @@
     handover.start()
     for copy in loads[7:]:
         copy.wait()
+    advance(ADVANCE[2])
     handover.wait_recv()
     in_recv[1 - core] = in_twin[...]
 
@@ -404,18 +393,14 @@
     def peer_rows(j):
         return pl.ds(pl.multiple_of(j * share, share), share)
 
-    started = []
-
     def to_peers(src, dst, s, r):
         for step in range(1, peers):
-            copy = remote(src(place.peer(step)), dst(step), s.at[step - 1], r.at[step - 1], {"tp": place.peer(step)})
-            copy.start()
-            started.append(copy)
-
-    to_peers(lambda j: att.at[peer_rows(j), :], lambda step: att_r.at[step - 1], rs1_s, rs1_r)
-    advance(ADVANCE[2])
-    for step in range(1, peers):
-        remote(att_r.at[step - 1], att_r.at[step - 1], rs1_s.at[step - 1], rs1_r.at[step - 1], {"tp": tp}).wait_recv()
+            remote(src(place.peer(step)), dst(step), s, r, {"tp": place.peer(step)}).start()
+
+    foreign = pl.ds(0, (peers - 1) * share)
+    to_peers(lambda j: att.at[peer_rows(j), :], lambda step: att_r.at[step - 1], tp_s.at[0], tp_r.at[0])
+    advance(ADVANCE[3])
+    wait_bytes(att_r, tp_r.at[0])
     total = att[peer_rows(tp), :].astype(F32)
     for step in range(1, peers):
         total = total + att_r[step - 1].astype(F32)
@@ -426,39 +411,11 @@
     normed = (values * multiplier * ng_ref[...].astype(F32).reshape(1, -1)).astype(BF16)
     nsend[...] = normed
     nall[peer_rows(tp), :] = normed
-    to_peers(lambda j: nsend, lambda step: nall.at[peer_rows(tp), :], ag_s, ag_r)
-    advance(ADVANCE[3])
-    for step in range(1, peers):
-        view = nall.at[peer_rows(place.peer(peers - step)), :]
-        remote(view, view, ag_s.at[step - 1], ag_r.at[step - 1], {"tp": tp}).wait_recv()
-    for slot in range(slots):
-        start = pl.multiple_of(place.slot_chip(slot) * LANE, LANE)
-        nperm[:, pl.ds(slot * LANE, LANE)] = nall[:, pl.ds(start, LANE)]
-
+    to_peers(lambda j: nsend, lambda step: nall.at[peer_rows(tp), :], tp_s.at[1], tp_r.at[1])
     advance(ADVANCE[4])
-    early = slots - 3
-    ready(gate_up, 0, early)
-    n_tile = 256 if (2 * half_w) % 256 == 0 else 128
-    head_k, tail_k = pl.ds(0, early * 2 * block), pl.ds(early * 2 * block, (slots - early) * 2 * block)
-
-    def tile_cols(n):
-        return pl.ds(pl.multiple_of(n * n_tile, n_tile), n_tile)
-
-    def project(n, _):
-        pre[:, tile_cols(n)] = nn(nperm[:, head_k], gu[head_k, tile_cols(n)])
-        return 0
-
-    lax.fori_loop(0, 2 * half_w // n_tile, project, 0)
-    ready(gate_up, early, slots)
-
-    def project_rest(n, _):
-        total = pre[:, tile_cols(n)] + nn(nperm[:, tail_k], gu[tail_k, tile_cols(n)])
-        pre[:, tile_cols(n)] = total.astype(BF16).astype(F32)
-        return 0
-
-    lax.fori_loop(0, 2 * half_w // n_tile, project_rest, 0)
-    halo_s[0] = pre[0:1, :]
-    halo_s[1] = pre[length - 1 : length, :]
+    wait_bytes(nall.at[foreign, :], tp_r.at[1])
+    halo_s[0] = nall[0:1, :].astype(F32)
+    halo_s[1] = nall[length - 1 : length, :].astype(F32)
     before, after = {"sp": place.span(-1)}, {"sp": place.span(1)}
     halos = [
         remote(halo_s.at[0], halo_r.at[1], halo_ss.at[0], halo_rs.at[1], before),
@@ -466,19 +423,54 @@
     ]
     for copy in halos:
         copy.start()
+    for slot in range(slots):
+        start = pl.multiple_of(place.slot_chip(slot) * LANE, LANE)
+        nperm[0:length, pl.ds(slot * LANE, LANE)] = nall[:, pl.ds(start, LANE)]
     advance(ADVANCE[5])
     for copy in halos:
         copy.wait_recv()
+    rim_row = lax.broadcasted_iota(jnp.int32, (RIM, LANE), 0)
     not_first = (sp > 0).astype(F32)
     not_last = (sp < spans - 1).astype(F32)
-
+    for slot in range(slots):
+        cols = pl.ds(pl.multiple_of(place.slot_chip(slot) * LANE, LANE), LANE)
+        rim = jnp.where(rim_row == 0, halo_r[0, :, cols] * not_first, 0.0)
+        rim = jnp.where(rim_row == 1, halo_r[1, :, cols] * not_last, rim)
+        nperm[pl.ds(length, RIM), pl.ds(slot * LANE, LANE)] = rim.astype(BF16)
+
+    ready(gate_up, 0)
+    n_tile = 256 if (2 * half_w) % 256 == 0 else 128
+    count = 2 * half_w // n_tile
+    split_at = early[0][1] * 2 * block
+    head_k, tail_k = pl.ds(0, split_at), pl.ds(split_at, spans * block - split_at)
+
+    def tile_cols(n):
+        return pl.ds(pl.multiple_of(n * n_tile, n_tile), n_tile)
+
+    def project(n, _):
+        pre[:, tile_cols(n)] = nn(nperm[:, head_k], gu[head_k, tile_cols(n)])
+        return 0
+
+    thirds = [count * n // 3 for n in range(4)]
+    for lo, hi in zip(thirds[:-1], thirds[1:]):
+        lax.fori_loop(lo, hi, project, 0)
+        advance(ADVANCE[6])
+    ready(gate_up, 1)
+
+    def project_rest(n, _):
+        total = pre[:, tile_cols(n)] + nn(nperm[:, tail_k], gu[tail_k, tile_cols(n)])
+        pre[:, tile_cols(n)] = total.astype(BF16).astype(F32)
+        return 0
+
+    lax.fori_loop(0, count, project_rest, 0)
+    advance(ADVANCE[7])
     def conv(n, _):
         results = []
         for base, taps in ((0, gt_ref), (half_w, ut_ref)):
             cols = pl.ds(pl.multiple_of(base + n * LANE, LANE), LANE)
-            x = pre[:, cols]
-            above = jnp.where(row == 0, halo_r[0, :, cols] * not_first, pltpu.roll(x, 1, 0))
-            below = jnp.where(row == length - 1, halo_r[1, :, cols] * not_last, pltpu.roll(x, length - 1, 0))
+            x = pre[0:length, cols]
+            above = jnp.where(row == 0, pre[pl.ds(length, 1), cols], pltpu.roll(x, 1, 0))
+            below = jnp.where(row == length - 1, pre[pl.ds(length + 1, 1), cols], pltpu.roll(x, length - 1, 0))
             t = taps[:, pl.ds(pl.multiple_of(n * LANE, LANE), LANE)].astype(F32)
             results.append(t[0:1] * above + t[1:2] * x + t[2:3] * below)
         gate, up = results
@@ -487,10 +479,8 @@
 
     lax.fori_loop(0, half_w // LANE, conv, 0)
 
-    cuts = sorted({0, slots // 2, slots - 2, slots})
-    pieces = list(zip(cuts[:-1], cuts[1:]))
-    for part_no, (lo, hi) in enumerate(pieces):
-        ready(down, lo, hi)
+    for part_no, (lo, hi) in enumerate(cuts):
+        ready(down, part_no)
 
         def project_down(n, _):
             rows_ = pl.ds(pl.multiple_of(n * 2 * LANE, 2 * LANE), 2 * LANE)
@@ -502,14 +492,12 @@
         to_peers(
             lambda j: ff.at[peer_rows(j), cols],
             lambda step: ff_r.at[step - 1, :, cols],
-            rs2_s.at[part_no],
-            rs2_r.at[part_no],
+            tp_s.at[2 + part_no],
+            tp_r.at[2 + part_no],
         )
-    for part_no, (lo, hi) in enumerate(pieces):
+    for part_no, (lo, hi) in enumerate(cuts):
         cols = pl.ds(lo * LANE, (hi - lo) * LANE)
-        for step in range(1, peers):
-            view = ff_r.at[step - 1, :, cols]
-            remote(view, view, rs2_s.at[part_no, step - 1], rs2_r.at[part_no, step - 1], {"tp": tp}).wait_recv()
+        wait_bytes(ff_r.at[:, :, cols], tp_r.at[2 + part_no])
         for slot in range(lo, hi):
             held = pl.ds(slot * LANE, LANE)
             home = pl.ds(pl.multiple_of(place.slot_chip(slot) * LANE, LANE), LANE)
@@ -519,10 +507,12 @@
             out_ref[:, home] = (mid[:, home].astype(F32) + total).astype(BF16)
 
     advance(10_000)
-    for copy in started + halos:
+    for copy in halos + swaps + [handover]:
         copy.wait_send()
-    for copy in swaps + [handover]:
-        copy.wait_send()
+    for n in range(2):
+        wait_bytes(att_r, tp_s.at[n])
+    for n, (lo, hi) in enumerate(cuts):
+        wait_bytes(ff_r.at[:, :, pl.ds(lo * LANE, (hi - lo) * LANE)], tp_s.at[2 + n])
     wait_bytes(st_send.at[others], a2a_s.at[0])
     wait_bytes(dec_recv.at[others], a2a_s.at[1])
     wait_bytes(in_send.at[others], a2a_s.at[2])
@@ -532,12 +522,15 @@
 
 PAIRED = True
 OWN_FIRST = 1
-RING_SHARE = 0.66
+GU_SHARE = 0.69
+DOWN_SHARE = 0.73
+RIM = 16
+EARLY = 1
 PAIR_LAG = 2
-DOWN_LAG = 1
+DOWN_LAG = 2
 GU_PARTS = 2
 DOWN_PARTS = 2
-ADVANCE = (4, 7, 4, 4, 0, 2)
+ADVANCE = (4, 7, 1, 5, 5, 0, 1, 1)
 
 
 def solution(mesh):
@@ -585,16 +578,17 @@
             pltpu.VMEM((share, width), BF16),
             pltpu.VMEM((share, width), BF16),
             pltpu.VMEM((length, width), BF16),
-            pltpu.VMEM((length, width), BF16),
-            pltpu.VMEM((length, 2 * half_w), F32),
-            pltpu.VMEM((2, 1, 2 * half_w), F32),
-            pltpu.VMEM((2, 1, 2 * half_w), F32),
+            pltpu.VMEM((length + RIM, width), BF16),
+            pltpu.VMEM((length + RIM, 2 * half_w), F32),
+            pltpu.VMEM((2, 1, width), F32),
+            pltpu.VMEM((2, 1, width), F32),
             pltpu.VMEM((length, half_w), BF16),
             pltpu.VMEM((length, width), BF16),
             pltpu.VMEM((peers - 1, share, width), BF16),
-            dma((14,)), dma((3,)), dma((3,)), dma((3,)), dma((3,)), dma((peers - 1,)), dma((peers - 1,)), dma((peers - 1,)), dma((peers - 1,)),
-            dma((2,)), dma((2,)), dma((3, peers - 1)), dma((3, peers - 1)),
-        ] + [dma((chips, n)) for n in (GU_PARTS, DOWN_PARTS) for _ in range(8)]
+            dma((14,)), dma((3,)), dma((3,)), dma((3,)), dma((3,)), dma((5,)), dma((5,)), dma((2,)), dma((2,)),
+        ]
+        for parts, held in zip((GU_PARTS, DOWN_PARTS), groups_of(chips)):
+            scratch += [dma((3,)), dma((chips, parts)), dma((chips // 2 + 1, parts)), dma((len(held),))]
         return pl.pallas_call(
             functools.partial(layer, groups, spans, peers),
             name="layer",

time: 121 us -> 112 us (0.926)
  Pallas kernels: 120 us -> 111 us
    pallas_call x1, Pallas kernels: 120 us -> 111 us  [shards(): pl.pallas_call(functools.partial(layer, groups, spans, peers), name='laye...]
where the time goes in v3:
time: 112 us
  Pallas kernels  111 us (99%)
  local copies, waits for them, and re-layouts  1.57 us (1%)
    pallas_call x1, Pallas kernels, shards(): pl.pallas_call(functools.partial(layer, groups, spans, peers), name='laye...  111 us

profile of v3, /device:TPU:33, one launch (start us, length us, event | category | flops | bytes accessed | tf_op | source)
XLA Modules:
  0.0 112.2 jit_solution(14730634147502131903)
XLA Ops:
  0.0 110.6 %layer.1 = bf16[32,2048]{1,0:T(8,128)(2,1)} custom-call(bf16[128,256]{1,0:T(8,128)(2,1)} %q_hbm.1, bf16[128,256]{1,0:T(8,128)(2,1)} %k_hbm.1, bf16[128,256]{1,0:T(8,128)(2,1)} %v_hbm.1, bf16[128,256]{1,0:T(8,128)(2,1)} %g_hbm.1, f32[2,2,128]{2,1,0:T(2,128)} %ld_hbm.1, f32[2,256]{1,0:T(2,128)} %hg_hbm.1, bf16[256,2048]{1,0:T(8,128)(2,1)} %wo_hbm.1, ...), custom_call_target="tpu_custom_call" | custom-call | tf_op jit(solution)/shard_map/layer/pallas_call | solution.py:592
  110.6 1.6 %copy.16 = bf16[32,2048]{1,0:T(8,128)(2,1)} copy(bf16[32,2048]{1,0:T(8,128)(2,1)} %layer.1) | data formatting | bytes 262144

commit v4 on v3

--- a/solution.py
+++ b/solution.py
@@ -30,7 +30,7 @@
 
 def groups_of(slots):
     early = slots - EARLY
-    cuts = sorted({0, slots // 2, slots - 2, slots})
+    cuts = sorted({0, slots // 2, slots - 4, slots - 2, slots})
     return [(0, early), (early, slots)], list(zip(cuts[:-1], cuts[1:]))
 
 
@@ -165,9 +165,7 @@
         wait_bytes(self.bulk(rest + self.block, self.width), self.twin_s)
 
 
-def order(gate_up, down, last):
-    late = []
-
+def order(gate_up, down, last, late):
     def one(stream, step, part):
         while len(late) > PAIR_LAG:
             a, b, c = late.pop(0)
@@ -186,7 +184,8 @@
             elif step > DOWN_LAG:
                 one(down, step - DOWN_LAG, part)
                 yield
-    for a, b, c in late:
+    while late:
+        a, b, c = late.pop(0)
         a.pair_tick(b, c)
 
 
@@ -210,10 +209,10 @@
 def layer(
     groups, spans, peers,
     q_hbm, k_hbm, v_hbm, g_hbm, ld_hbm, hg_hbm, wo_hbm, res_hbm, ng_hbm, gw_hbm, uw_hbm, dw_hbm, gt_hbm, ut_hbm,
-    out_ref,
+    out_hbm,
     q_ref, k_ref, v_ref, g_ref, ld_ref, hg_ref, ng_ref, gt_ref, ut_ref, gu, dn, wo, res, st, st_twin, dec, dec_twin, st_send, st_recv, dec_send, dec_recv, in_send, in_recv, in_twin, inner, grow, mix, att, att_r,
-    mid, nsend, nall, nperm, pre, halo_s, halo_r, hid, ff, ff_r,
-    load_sem, twin_s, twin_r, a2a_s, a2a_r, tp_s, tp_r, halo_ss, halo_rs,
+    mid, nsend, nall, nperm, pre, halo_s, halo_r, hid, ff, ff_r, pair_sum, out_ref,
+    load_sem, out_sem, twin_s, twin_r, a2a_s, a2a_r, tp_s, tp_r, mid_r, halo_ss, halo_rs,
     gu_s, gu_ring, gu_pair, gu_twin, dn_s, dn_ring, dn_pair, dn_twin,
 ):
     place = Place(groups, spans, peers)
@@ -293,14 +292,16 @@
     early, cuts = groups_of(slots)
     gate_up = Stream(place, gu, GU_SHARE, GU_PARTS, early, gu_s, gu_ring, gu_pair, gu_twin)
     down = Stream(place, dn, DOWN_SHARE, DOWN_PARTS, cuts, dn_s, dn_ring, dn_pair, dn_twin)
-    ring = order(gate_up, down, place.chips // 2)
+    late = []
+    ring = order(gate_up, down, place.chips // 2, late)
 
     def advance(n):
         for _ in range(n):
             next(ring, None)
 
     def ready(stream, group):
-        while not stream.handed.issuperset(range(*stream.groups[group])):
+        wanted = set(range(*stream.groups[group]))
+        while not stream.handed >= wanted:
             next(ring, None)
         stream.ready(group)
 
@@ -462,8 +463,10 @@
         pre[:, tile_cols(n)] = total.astype(BF16).astype(F32)
         return 0
 
-    lax.fori_loop(0, count, project_rest, 0)
+    lax.fori_loop(0, count // 2, project_rest, 0)
     advance(ADVANCE[7])
+    lax.fori_loop(count // 2, count, project_rest, 0)
+    advance(ADVANCE[8])
     def conv(n, _):
         results = []
         for base, taps in ((0, gt_ref), (half_w, ut_ref)):
@@ -478,6 +481,30 @@
         return 0
 
     lax.fori_loop(0, half_w // LANE, conv, 0)
+    advance(ADVANCE[9])
+
+    right, left = {"tp": place.peer(1)}, {"tp": place.peer(peers - 1)}
+
+    def sides(lo, hi):
+        middle = (lo + hi) // 2
+        first, second = pl.ds(lo * LANE, (middle - lo) * LANE), pl.ds(middle * LANE, (hi - middle) * LANE)
+        return (0, first, second, right, place.peer(1)), (1, second, first, left, place.peer(peers - 1))
+
+    def around_first(n, lo, hi):
+        for plane, shared, alone, device, to in sides(lo, hi):
+            far = ff.at[peer_rows(place.peer(2)), shared]
+            remote(far, ff_r.at[2, :, shared], tp_s.at[2 + n], mid_r.at[n], device).start()
+            near = ff.at[peer_rows(to), alone]
+            remote(near, ff_r.at[plane, :, alone], tp_s.at[2 + n], tp_r.at[2 + n], device).start()
+
+    def around_second(n, lo, hi):
+        wait_bytes(ff_r.at[2, :, pl.ds(lo * LANE, (hi - lo) * LANE)], mid_r.at[n])
+        for plane, shared, alone, device, to in sides(lo, hi):
+            total = ff[peer_rows(to), shared].astype(F32) + ff_r[2, :, shared].astype(F32)
+            pair_sum[plane, :, shared] = total.astype(BF16)
+            remote(
+                pair_sum.at[plane, :, shared], ff_r.at[plane, :, shared], tp_s.at[2 + n], tp_r.at[2 + n], device
+            ).start()
 
     for part_no, (lo, hi) in enumerate(cuts):
         ready(down, part_no)
@@ -489,22 +516,32 @@
 
         lax.fori_loop(lo // 2, hi // 2, project_down, 0)
         cols = pl.ds(lo * LANE, (hi - lo) * LANE)
-        to_peers(
-            lambda j: ff.at[peer_rows(j), cols],
-            lambda step: ff_r.at[step - 1, :, cols],
-            tp_s.at[2 + part_no],
-            tp_r.at[2 + part_no],
-        )
+        if AROUND and peers == 4:
+            around_first(part_no, lo, hi)
+        else:
+            to_peers(
+                lambda j: ff.at[peer_rows(j), cols],
+                lambda step: ff_r.at[step - 1, :, cols],
+                tp_s.at[2 + part_no],
+                tp_r.at[2 + part_no],
+            )
+    if AROUND and peers == 4:
+        for part_no, (lo, hi) in enumerate(cuts):
+            around_second(part_no, lo, hi)
     for part_no, (lo, hi) in enumerate(cuts):
         cols = pl.ds(lo * LANE, (hi - lo) * LANE)
-        wait_bytes(ff_r.at[:, :, cols], tp_r.at[2 + part_no])
+        arriving = 2 if AROUND and peers == 4 else peers - 1
+        wait_bytes(ff_r.at[pl.ds(0, arriving), :, cols], tp_r.at[2 + part_no])
         for slot in range(lo, hi):
             held = pl.ds(slot * LANE, LANE)
             home = pl.ds(pl.multiple_of(place.slot_chip(slot) * LANE, LANE), LANE)
             total = ff[peer_rows(tp), held].astype(F32)
-            for step in range(1, peers):
-                total = total + ff_r[step - 1, :, held].astype(F32)
+            for step in range(arriving):
+                total = total + ff_r[step, :, held].astype(F32)
             out_ref[:, home] = (mid[:, home].astype(F32) + total).astype(BF16)
+        for slot in range(lo, hi):
+            home = pl.ds(pl.multiple_of(place.slot_chip(slot) * LANE, LANE), LANE)
+            pltpu.make_async_copy(out_ref.at[:, home], out_hbm.at[:, home], out_sem).start()
 
     advance(10_000)
     for copy in halos + swaps + [handover]:
@@ -518,19 +555,21 @@
     wait_bytes(in_send.at[others], a2a_s.at[2])
     gate_up.drain()
     down.drain()
+    wait_bytes(out_ref, out_sem)
 
 
 PAIRED = True
 OWN_FIRST = 1
+AROUND = False
 GU_SHARE = 0.69
-DOWN_SHARE = 0.73
+DOWN_SHARE = 0.66
 RIM = 16
 EARLY = 1
 PAIR_LAG = 2
-DOWN_LAG = 2
+DOWN_LAG = 1
 GU_PARTS = 2
 DOWN_PARTS = 2
-ADVANCE = (4, 7, 1, 5, 5, 0, 1, 1)
+ADVANCE = (4, 7, 1, 5, 5, 2, 1, 1, 0, 1)
 
 
 def solution(mesh):
@@ -552,7 +591,6 @@
         chips = spans // 2
         packet = 2 * HEAD // chips
         dma = pltpu.SemaphoreType.DMA
-        vmem = pl.BlockSpec(memory_space=pltpu.VMEM)
         hbm = pl.BlockSpec(memory_space=pltpu.HBM)
         scratch = [pltpu.VMEM(a.shape, a.dtype) for a in (q, k, v, g, ld, hg, ng, gt, ut)] + [
             pltpu.VMEM((spans * block, 2 * half_w), BF16),
@@ -585,7 +623,9 @@
             pltpu.VMEM((length, half_w), BF16),
             pltpu.VMEM((length, width), BF16),
             pltpu.VMEM((peers - 1, share, width), BF16),
-            dma((14,)), dma((3,)), dma((3,)), dma((3,)), dma((3,)), dma((5,)), dma((5,)), dma((2,)), dma((2,)),
+            pltpu.VMEM((2, share, width), BF16),
+            pltpu.VMEM((share, width), BF16),
+            dma((14,)), dma, dma((3,)), dma((3,)), dma((3,)), dma((3,)), dma((6,)), dma((6,)), dma((4,)), dma((2,)), dma((2,)),
         ]
         for parts, held in zip((GU_PARTS, DOWN_PARTS), groups_of(chips)):
             scratch += [dma((3,)), dma((chips, parts)), dma((chips // 2 + 1, parts)), dma((len(held),))]
@@ -594,7 +634,7 @@
             name="layer",
             out_shape=jax.ShapeDtypeStruct((share, width), BF16),
             in_specs=[hbm] * 14,
-            out_specs=vmem,
+            out_specs=hbm,
             scratch_shapes=scratch,
             compiler_params=pltpu.CompilerParams(
                 collective_id=0, has_side_effects=True, vmem_limit_bytes=67_043_328

time: 112 us -> 110 us (0.982)
  Pallas kernels: 111 us -> 108 us
    pallas_call x1, Pallas kernels: 111 us -> 108 us  [shards(): pl.pallas_call(functools.partial(layer, groups, spans, peers), name='laye...]
where the time goes in v4:
time: 110 us
  Pallas kernels  108 us (98%)
  local copies, waits for them, and re-layouts  1.57 us (1%)
    pallas_call x1, Pallas kernels, shards(): pl.pallas_call(functools.partial(layer, groups, spans, peers), name='laye...  108 us

profile of v4, /device:TPU:33, one launch (start us, length us, event | category | flops | bytes accessed | tf_op | source)
XLA Modules:
  0.0 109.8 jit_solution(94902720718593521)
XLA Ops:
  0.0 108.3 %layer.1 = bf16[32,2048]{1,0:T(8,128)(2,1)} custom-call(bf16[128,256]{1,0:T(8,128)(2,1)} %q_hbm.1, bf16[128,256]{1,0:T(8,128)(2,1)} %k_hbm.1, bf16[128,256]{1,0:T(8,128)(2,1)} %v_hbm.1, bf16[128,256]{1,0:T(8,128)(2,1)} %g_hbm.1, f32[2,2,128]{2,1,0:T(2,128)} %ld_hbm.1, f32[2,256]{1,0:T(2,128)} %hg_hbm.1, bf16[256,2048]{1,0:T(8,128)(2,1)} %wo_hbm.1, ...), custom_call_target="tpu_custom_call" | custom-call | tf_op jit(solution)/shard_map/layer/pallas_call | solution.py:632
  108.3 1.6 %copy.16 = bf16[32,2048]{1,0:T(8,128)(2,1)} copy(bf16[32,2048]{1,0:T(8,128)(2,1)} %layer.1) | data formatting | bytes 262144

commit v5 on v4

--- a/solution.py
+++ b/solution.py
@@ -94,6 +94,10 @@
         start = pl.multiple_of(slot * 2 * self.block + self.p.core * self.block + part * self.rows, self.rows)
         return self.buf.at[pl.ds(start, self.rows), cols]
 
+    def whole(self, slot, cols):
+        start = pl.multiple_of(slot * 2 * self.block + self.p.core * self.block, self.block)
+        return self.buf.at[pl.ds(start, self.block), cols]
+
     def bulk(self, rows, width):
         return self.buf.at[pl.ds(0, rows), pl.ds(0, width)]
 
@@ -108,15 +112,16 @@
         src, dst = self.view(src_slot, part, cols), self.view(dst_slot, part, cols)
         remote(src, dst, self.ring_s, self.ring_r.at[dst_slot, part], self.p.along(way)).start()
 
-    def to_twin(self, slot, part, cols):
-        view = self.view(slot, part, cols)
+    def to_twin(self, slot, cols):
+        view = self.whole(slot, cols)
         group = [n for n, (lo, hi) in enumerate(self.groups) if lo <= slot < hi][0]
         remote(view, view, self.twin_s, self.twin_r.at[group], self.p.twin).start()
 
     def own(self, part):
         self.on(0, 1, part, 1)
         self.on(0, 2, part, -1)
-        self.to_twin(0, part, pl.ds(0, self.width))
+        if part == self.parts - 1:
+            self.to_twin(0, pl.ds(0, self.width))
 
     def got(self, slot, part):
         view = self.view(slot, part, self.ring_cols())
@@ -136,22 +141,25 @@
                 self.got(behind, part)
                 self.got(ahead, part)
                 self.on(behind + self.p.core, self.opposite, part, 1 - 2 * self.p.core)
+        if part < self.parts - 1:
+            return
         for slot in self.slots(step):
             if self.p.paired:
-                view = self.view(slot, part, pl.ds(self.give_o, self.pair_w))
-                remote(view, view, self.pair_s, self.pair_r.at[step, part], self.p.pair).start()
+                view = self.whole(slot, pl.ds(self.give_o, self.pair_w))
+                remote(view, view, self.pair_s, self.pair_r.at[step], self.p.pair).start()
         for slot in self.slots(step):
-            self.to_twin(slot, part, self.ring_cols())
+            self.to_twin(slot, self.ring_cols())
 
     def pair_tick(self, step, part):
+        if part < self.parts - 1:
+            return
         slots = self.slots(step)
-        if part == self.parts - 1:
-            self.handed.update(slots)
+        self.handed.update(slots)
         if not self.p.paired:
             return
-        wait_bytes(self.bulk(len(slots) * self.rows, self.pair_w), self.pair_r.at[step, part])
+        wait_bytes(self.bulk(len(slots) * self.block, self.pair_w), self.pair_r.at[step])
         for slot in slots:
-            self.to_twin(slot, part, pl.ds(self.pair_o, self.pair_w))
+            self.to_twin(slot, pl.ds(self.pair_o, self.pair_w))
 
     def ready(self, group):
         lo, hi = self.groups[group]
@@ -628,7 +636,7 @@
             dma((14,)), dma, dma((3,)), dma((3,)), dma((3,)), dma((3,)), dma((6,)), dma((6,)), dma((4,)), dma((2,)), dma((2,)),
         ]
         for parts, held in zip((GU_PARTS, DOWN_PARTS), groups_of(chips)):
-            scratch += [dma((3,)), dma((chips, parts)), dma((chips // 2 + 1, parts)), dma((len(held),))]
+            scratch += [dma((3,)), dma((chips, parts)), dma((chips // 2 + 1,)), dma((len(held),))]
         return pl.pallas_call(
             functools.partial(layer, groups, spans, peers),
             name="layer",

time: 110 us -> 113 us (1.027)
  Pallas kernels: 108 us -> 111 us
    pallas_call x1, Pallas kernels: 108 us -> 111 us  [shards(): pl.pallas_call(functools.partial(layer, groups, spans, peers), name='laye...]
where the time goes in v5:
time: 113 us; the launch traced here: 112 us
  Pallas kernels  111 us (98%)
  local copies, waits for them, and re-layouts  1.57 us (1%)
    pallas_call x1, Pallas kernels, shards(): pl.pallas_call(functools.partial(layer, groups, spans, peers), name='laye...  111 us

profile of v5, /device:TPU:33, one launch (start us, length us, event | category | flops | bytes accessed | tf_op | source)
XLA Modules:
  0.0 112.3 jit_solution(7592617217649378144)
XLA Ops:
  0.0 110.8 %layer.1 = bf16[32,2048]{1,0:T(8,128)(2,1)} custom-call(bf16[128,256]{1,0:T(8,128)(2,1)} %q_hbm.1, bf16[128,256]{1,0:T(8,128)(2,1)} %k_hbm.1, bf16[128,256]{1,0:T(8,128)(2,1)} %v_hbm.1, bf16[128,256]{1,0:T(8,128)(2,1)} %g_hbm.1, f32[2,2,128]{2,1,0:T(2,128)} %ld_hbm.1, f32[2,256]{1,0:T(2,128)} %hg_hbm.1, bf16[256,2048]{1,0:T(8,128)(2,1)} %wo_hbm.1, ...), custom_call_target="tpu_custom_call" | custom-call | tf_op jit(solution)/shard_map/layer/pallas_call | solution.py:640
  110.8 1.6 %copy.16 = bf16[32,2048]{1,0:T(8,128)(2,1)} copy(bf16[32,2048]{1,0:T(8,128)(2,1)} %layer.1) | data formatting | bytes 262144
